TPU v7x, 512 devices: a whole 4x4x16 slice. The times are simulated.
512 devices in a mesh: sp: 32 (over z, core), tp: 16 (over y, x).
Axes of the slice: x: 4, y: 4, z: 16, core: 2. Of those that a mesh axis runs over, the one named last changes fastest.
Arguments:
- residual: bfloat16 [4096, 2048], P('sp', 'tp'), may hold values from -6 to 6
- out_cot: bfloat16 [4096, 2048], P('sp', 'tp'), may hold values from -6 to 6
- routes: int32 [4096, 2], P('sp'), may hold values from 0 to 31, all different within a row; in each aligned block of 128 rows (0 to 127, 128 to 255, ...) at most 10 rows name the same one
- route_weight: float32 [4096, 2], P('sp'), may hold values from 0.2 to 1
- w_gate: bfloat16 [32, 2048, 2048], P('sp', 'tp'), may hold values from -0.125 to 0.125
- w_up: bfloat16 [32, 2048, 2048], P('sp', 'tp'), may hold values from -0.125 to 0.125
- w_down: bfloat16 [32, 2048, 2048], P('sp', 'tp'), may hold values from -0.125 to 0.125
- w_out: bfloat16 [1024, 2048], P('tp'), may hold values from -0.1875 to 0.1875
- conv_out: bfloat16 [1024, 4096], P('tp', 'sp'), may hold values from -14 to 14
- gate_branch: bfloat16 [1024, 4096], P('tp', 'sp'), may hold values from -6 to 6
- w_recur: bfloat16 [16, 64, 64], P('tp'), may hold values from -0.75 to 0.75
- w_input: bfloat16 [16, 64, 64], P('tp'), may hold values from -0.75 to 0.75
- decay_param: float32 [1024], P('tp'), may hold values from 4.5 to 11
Outputs:
- grad_gate: bfloat16 [32, 2048, 2048], P('sp', 'tp')
- grad_up: bfloat16 [32, 2048, 2048], P('sp', 'tp')
- grad_down: bfloat16 [32, 2048, 2048], P('sp', 'tp')
- grad_proj: float32 [2048, 1024], P('sp', 'tp')
- grad_conv: float32 [1024, 4096], P('tp', 'sp')
- grad_branch: float32 [1024, 4096], P('tp', 'sp')
Inputs may be any that keep to these rules, and one draw needn't show every extreme that they name: `routes`: in the rows of one index of sp no expert is named more than 10 times, a bound that some block reaches.
All inputs are finite; a program needn't handle non-finite values.
Results may differ from a plain program's by a relative error of at most 0.025.
Values may be sent and summed in bfloat16 or wider, within the bound.
No kernel may reach another device: no remote copies, remote signals or barrier semaphores. Data moves between devices by JAX's collectives and lax.ppermute only.
A program may use at most 64 MiB of HBM per device.

v0:
```python
import jax
import jax.numpy as jnp
from jax import lax
from jax.experimental import pallas as pl
from jax.experimental.pallas import tpu as pltpu
from jax.sharding import PartitionSpec as P

LEAK = 0.01
DECAY_SCALE = 8.0
GELU_A = 0.7978845608028654
GELU_B = 0.044715

BF = jnp.bfloat16
F32 = jnp.float32
I32 = jnp.int32

SEND_ROWS = 24
HOME_ROWS = 16
LAST_ROWS = 40


def iota(shape, dim):
    return lax.broadcasted_iota(I32, shape, dim)


def dot(a, b, ca=1, cb=0, precision=None):
    return lax.dot_general(
        a, b, (((ca,), (cb,)), ((), ())), precision=precision, preferred_element_type=F32
    )


def call(body, outs, args, flops=1, bytes_moved=1, scalars=0, scratch=()):
    specs = [pl.BlockSpec(memory_space=pltpu.SMEM)] * scalars
    specs += [pl.BlockSpec(memory_space=pltpu.VMEM)] * (len(args) - scalars)
    return pl.pallas_call(
        body,
        out_shape=[jax.ShapeDtypeStruct(s, d) for s, d in outs],
        in_specs=specs,
        out_specs=[pl.BlockSpec(memory_space=pltpu.VMEM)] * len(outs),
        scratch_shapes=list(scratch),
        compiler_params=pltpu.CompilerParams(vmem_limit_bytes=24 * 1024 * 1024),
        cost_estimate=pl.CostEstimate(
            flops=flops, bytes_accessed=bytes_moved, transcendentals=0
        ),
    )(*args)


def dispatch_body(experts, routes, weight, residual, cot, sent, comb):
    tokens = residual.shape[0]
    first, second = routes[0:1, :], routes[1:2, :]
    expert = iota((experts, tokens), 0)
    hit0 = (expert == first).astype(F32)
    hit1 = (expert == second).astype(F32)
    earlier = (iota((tokens, tokens), 0) < iota((tokens, tokens), 1)).astype(BF)
    before = dot((hit0 + hit1).astype(BF), earlier)
    slot0 = jnp.sum(before * hit0, axis=0, keepdims=True).astype(I32)
    slot1 = jnp.sum((before + hit0) * hit1, axis=0, keepdims=True).astype(I32)
    back = iota((experts * HOME_ROWS, tokens), 0)
    at_home = (back == first * HOME_ROWS + slot0) | (back == second * HOME_ROWS + slot1)
    comb[...] = at_home.astype(F32).astype(BF)
    row = iota((experts * SEND_ROWS, tokens), 0)
    place0 = first * SEND_ROWS + slot0
    place1 = second * SEND_ROWS + slot1
    in_rows = ((row == place0) | (row == place1)).astype(F32).astype(BF)
    capacity = SEND_ROWS // 2 - 2
    cot0 = row == place0 + capacity
    cot1 = row == place1 + capacity
    factor = jnp.sum(
        jnp.where(cot0, weight[0:1, :], 0.0) + jnp.where(cot1, weight[1:2, :], 0.0),
        axis=1,
        keepdims=True,
    )
    cot_rows = (cot0 | cot1).astype(F32).astype(BF)
    rows = dot(in_rows, residual[...]) + factor * dot(cot_rows, cot[...])
    sent[...] = rows.astype(BF)


def compact_body(experts, capacity, got, out):
    slots = experts * capacity
    total = got.shape[0]
    row = iota((2 * slots, 1), 0)
    half = (row >= slots).astype(I32)
    rest = row - half * slots
    source = jnp.floor((rest.astype(F32) + 0.5) * (1.0 / capacity)).astype(I32)
    target = source * SEND_ROWS + half * capacity + (rest - source * capacity)
    pick = (iota((2 * slots, total), 1) == target).astype(F32).astype(BF)
    rows = dot(pick, got[...]).astype(BF)
    for j in range(out.shape[0]):
        out[j] = rows


def pair(ref, k, lo, hi):
    return jnp.concatenate([ref[2 * k, lo:hi, :], ref[2 * k + 1, lo:hi, :]], axis=1)


def expert_body(whole, w_gate, w_up, w_down, dxp, acts):
    slots = whole.shape[1] // 2
    blocks = whole.shape[0]
    hidden = w_gate.shape[0]
    pre = jnp.zeros((slots, 2 * hidden), F32)
    act_cot = jnp.zeros((slots, hidden), F32)
    for k in range(blocks // 2):
        cols = slice(256 * k, 256 * (k + 1))
        both = jnp.concatenate([w_gate[:, cols], w_up[:, cols]], axis=0)
        pre = pre + dot(pair(whole, k, 0, slots), both, 1, 1)
        act_cot = act_cot + dot(pair(whole, k, slots, 2 * slots), w_down[:, cols], 1, 1)
    pre_gate, pre_up = pre[:, :hidden], pre[:, hidden:]
    sig = jax.nn.sigmoid(pre_gate)
    silu = pre_gate * sig
    slope = sig * (1.0 + pre_gate * (1.0 - sig))
    act = (silu * pre_up).astype(BF)
    gate_cot = (act_cot * pre_up * slope).astype(BF)
    up_cot = (act_cot * silu).astype(BF)
    cots = jnp.concatenate([gate_cot, up_cot], axis=1)
    acts[:, : 2 * hidden] = cots
    acts[:, 2 * hidden :] = act
    for k in range(blocks // 2):
        cols = slice(256 * k, 256 * (k + 1))
        both = jnp.concatenate([w_gate[:, cols], w_up[:, cols]], axis=0)
        part = dot(cots, both).astype(BF)
        dxp[2 * k] = part[:, :128]
        dxp[2 * k + 1] = part[:, 128:]


def grads_body(whole, acts, g_gate, g_up, g_down):
    slots = whole.shape[1] // 2
    hidden = acts.shape[1] // 3
    both = dot(acts[:, : 2 * hidden], pair(whole, 0, 0, slots), 0, 0).astype(BF)
    g_gate[0] = both[:hidden]
    g_up[0] = both[hidden:]
    g_down[0] = dot(acts[:, 2 * hidden :], pair(whole, 0, slots, 2 * slots), 0, 0).astype(BF)


def expert_grads(whole, acts, width):
    blocks, rows, lanes = whole.shape
    hidden = acts.shape[1] // 3
    out = jax.ShapeDtypeStruct((1, hidden, width), BF)
    spec = pl.BlockSpec((1, hidden, 2 * lanes), lambda i: (0, 0, i))
    return pl.pallas_call(
        grads_body,
        grid=(blocks // 2,),
        out_shape=[out] * 3,
        in_specs=[
            pl.BlockSpec((2, rows, lanes), lambda i: (i, 0, 0)),
            pl.BlockSpec(acts.shape, lambda i: (0, 0)),
        ],
        out_specs=[spec] * 3,
        compiler_params=pltpu.CompilerParams(vmem_limit_bytes=16 * 1024 * 1024),
        cost_estimate=pl.CostEstimate(
            flops=3 * rows * hidden * width, bytes_accessed=6 * hidden * width, transcendentals=0
        ),
    )(whole, acts)


def owner_sum_body(experts, capacity, parts, carry, out):
    total = parts[0].astype(F32)
    for j in range(1, parts.shape[0]):
        total = total + parts[j].astype(F32)
    total = total.astype(BF)
    rows = experts * HOME_ROWS
    place = iota((rows, 1), 0)
    inner = place & (HOME_ROWS - 1)
    source = jnp.where(inner < capacity, (place >> 4) * capacity + inner, -1)
    pick = (iota((rows, experts * capacity), 1) == source).astype(F32).astype(BF)
    extra = (iota((rows, carry.shape[0]), 1) == inner - capacity).astype(F32).astype(BF)
    out[...] = (dot(pick, total) + dot(extra, carry[...])).astype(BF)


def lift_body(home, comb, cot, out):
    grad = dot(comb[...], home[...], 0, 0)
    lifted = (cot[...].astype(F32) + grad).astype(BF)
    for j in range(out.shape[0]):
        out[j] = lifted


def shift_in(x, d, fill, lane):
    return jnp.where(lane >= d, pltpu.roll(x, d, 1), fill)


def shift_out(x, d, fill, lane):
    width = x.shape[1]
    return jnp.where(lane < width - d, pltpu.roll(x, width - d, 1), fill)


def scan(decay, drive, lane, moved):
    d = 1
    while d < decay.shape[1]:
        drive = decay * moved(drive, d, 0.0, lane) + drive
        decay = decay * moved(decay, d, 1.0, lane)
        d *= 2
    return decay, drive


def in_three(x):
    high = x.astype(BF)
    rest = x - high.astype(F32)
    mid = rest.astype(BF)
    low = (rest - mid.astype(F32)).astype(BF)
    return high, mid, low


def ends_row(up, down, lane):
    width = up.shape[1]
    ends = jnp.concatenate(
        [jnp.where(lane == width - 1, up, 0.0), jnp.where(lane == 0, down, 0.0)], axis=0
    )
    return dot(jnp.ones((8, width), F32), ends, 1, 1, lax.Precision.HIGHEST)


def to_columns(row, lane):
    channel = iota(lane.shape, 0)
    channels = lane.shape[0]
    up = jnp.sum(jnp.where(lane == channel, row, 0.0), axis=1, keepdims=True)
    down = jnp.sum(jnp.where(lane == channel + channels, row, 0.0), axis=1, keepdims=True)
    return up, down


def fold(me, prods, adds, channels):
    devices, width = prods.shape
    lane = iota((1, width), 1)
    ahead = lane < channels
    total = jnp.zeros((1, width), F32)
    for n in range(devices):
        m = devices - 1 - n
        prod = jnp.where(ahead, prods[n : n + 1, :], prods[m : m + 1, :])
        add = jnp.where(ahead, adds[n : n + 1, :], adds[m : m + 1, :])
        live = jnp.where(ahead, (me > n).astype(I32), (me < m).astype(I32)) > 0
        total = jnp.where(live, prod * total + add, total)
    return total


SAVED = 11


def state_body(conv, branch, w_recur, w_input, soft, saved, carry):
    channels, tokens = conv.shape
    lane = iota((channels, tokens), 1)
    eye = iota((channels, channels), 0) == iota((channels, channels), 1)
    softness = jnp.sum(jnp.where(eye, soft[...], 0.0), axis=1, keepdims=True)
    values = conv[...].astype(F32)
    sig_r = jax.nn.sigmoid(dot(w_recur[0], conv[...], 0, 0))
    sig_a = jax.nn.sigmoid(dot(w_input[0], conv[...], 0, 0))
    decay = jnp.exp(-DECAY_SCALE * sig_r * softness)
    root = jnp.sqrt(1.0 - decay * decay + LEAK)
    direct = root * sig_a
    drive = direct * values
    up_prod, up_state = scan(decay, drive, lane, shift_in)
    down_prod, down_state = scan(decay, drive, lane, shift_out)
    x = branch[...].astype(F32)
    th = jnp.tanh(GELU_A * (x + GELU_B * x * x * x))
    saved[0] = decay
    saved[1] = up_prod
    saved[2] = up_state
    saved[3] = down_prod
    saved[4] = down_state
    saved[5] = 0.5 * x * (1.0 + th)
    saved[6] = 0.5 * (1.0 + th) + 0.5 * x * (1.0 - th * th) * GELU_A * (
        1.0 + 3.0 * GELU_B * x * x
    )
    saved[7] = decay * (-DECAY_SCALE * softness) * sig_r * (1.0 - sig_r)
    saved[8] = -(decay / root) * sig_a * values
    saved[9] = root * values * sig_a * (1.0 - sig_a)
    saved[10] = direct
    rows = in_three(ends_row(up_prod, down_prod, lane)) + in_three(
        ends_row(up_state, down_state, lane)
    )
    place = iota((8, tokens), 0)
    total = jnp.zeros((8, tokens), F32)
    for k, row in enumerate(rows):
        total = jnp.where(place == k, row.astype(F32), total)
    carry[...] = total.astype(BF)


def join_body(me, home, saved, mix, joined, prods, adds):
    devices = prods.shape[0]
    channels, tokens = mix.shape
    rows = home.shape[0]
    lane = iota((channels, tokens), 1)
    offset = iota((devices, rows), 1) - HOME_ROWS * iota((devices, rows), 0)
    base = HOME_ROWS - 6
    prod_rows = ((offset >= base) & (offset < base + 3)).astype(F32).astype(BF)
    add_rows = ((offset >= base + 3) & (offset < base + 6)).astype(F32).astype(BF)
    prods[...] = dot(prod_rows, home[...])
    adds[...] = dot(add_rows, home[...])
    state_in, state_back = to_columns(fold(me[0], prods, adds, channels), lane)
    fwd = saved[2] + saved[1] * state_in
    bwd = saved[4] + saved[3] * state_back
    total = fwd + bwd
    mix[...] = (saved[5] * total).astype(BF)
    joined[0] = jnp.where(lane == 0, state_in, pltpu.roll(fwd, 1, 1))
    joined[1] = jnp.where(lane == tokens - 1, state_back, pltpu.roll(bwd, tokens - 1, 1))
    joined[2] = total * saved[6]


def last_body(lifted, w_out, mix, saved, out, kept):
    blocks, tokens, _ = lifted.shape
    channels = mix.shape[0]
    half = channels // 2
    lane = iota((channels, tokens), 1)
    left = iota((half, 128), 1) < 64
    mixed = mix[...]
    mix_cot = jnp.zeros((channels, tokens), F32)
    for k in range(blocks // 2):
        both = pair(lifted, k, 0, tokens)
        mix_cot = mix_cot + dot(w_out[:, 256 * k : 256 * (k + 1)], both, 1, 1)
        proj = dot(mixed, both)
        for q in range(2):
            part = proj[:, 128 * q : 128 * (q + 1)]
            top, bottom = part[:half], part[half:]
            spot = 4 * k + 2 * q
            out[spot, :half, :] = jnp.where(left, top, pltpu.roll(bottom, 64, 1)).astype(BF)
            out[spot + 1, :half, :] = jnp.where(left, pltpu.roll(top, 64, 1), bottom).astype(BF)
    decay = saved[0]
    cot = mix_cot * saved[5]
    weighted = decay * cot
    _, up = scan(decay, weighted, lane, shift_in)
    _, down = scan(decay, weighted, lane, shift_out)
    kept[0] = mix_cot
    kept[1] = cot
    kept[2] = up
    kept[3] = down
    rows = in_three(ends_row(up, down, lane))
    place = iota((8, tokens), 0)
    total = jnp.zeros((8, tokens), F32)
    for k, row in enumerate(rows):
        total = jnp.where(place == k, row.astype(F32), total)
    total = total.astype(BF)
    for s in range(out.shape[0]):
        out[s, half:, :] = total


def finish_body(me, last, prods, saved, joined, kept, w_recur, w_input, g_proj, g_conv, g_branch, adds):
    devices = prods.shape[0]
    channels, tokens = g_conv.shape
    half = channels // 2
    lane = iota((channels, tokens), 1)
    total = last[0, :half, :].astype(F32)
    carry = jnp.zeros((8, tokens), F32)
    for s in range(devices):
        if s:
            total = total + last[s, :half, :].astype(F32)
        adds[s : s + 1, :] = jnp.sum(last[s, half:, :].astype(F32), axis=0, keepdims=True)
    turned = total.T
    g_proj[...] = jnp.concatenate([turned[:64], turned[64:]], axis=1)
    adj_in, adj_back = to_columns(fold(me[0], prods, adds, channels), lane)
    cot = kept[1]
    up = kept[2] + saved[1] * adj_in
    down = kept[3] + saved[3] * adj_back
    past = cot + jnp.where(lane == 0, adj_in, pltpu.roll(up, 1, 1))
    future = cot + jnp.where(lane == tokens - 1, adj_back, pltpu.roll(down, tokens - 1, 1))
    drive_cot = past + future
    decay_cot = future * joined[0] + past * joined[1] + drive_cot * saved[8]
    recur_cot = decay_cot * saved[7]
    admit_cot = drive_cot * saved[9]
    exact = lax.Precision.HIGHEST
    g_conv[...] = (
        drive_cot * saved[10]
        + dot(w_recur[0].astype(F32), recur_cot, 1, 0, exact)
        + dot(w_input[0].astype(F32), admit_cot, 1, 0, exact)
    )
    g_branch[...] = kept[0] * joined[2]


def local(
    residual,
    out_cot,
    routes,
    route_weight,
    w_gate,
    w_up,
    w_down,
    w_out,
    conv_out,
    gate_branch,
    w_recur,
    w_input,
    decay_param,
):
    experts = lax.axis_size("sp")
    blocks = lax.axis_size("tp")
    me = lax.axis_index("sp").reshape(1).astype(I32)
    tokens, lanes = residual.shape
    capacity = 2 * tokens // experts + 2
    slots = experts * capacity
    hidden, width = w_gate.shape[1:]
    channels = conv_out.shape[0]

    def kernel(body, *static):
        def run(*refs):
            body(*static, *refs)

        return run

    sent, comb = call(
        kernel(dispatch_body, experts),
        [((experts * SEND_ROWS, lanes), BF), ((experts * HOME_ROWS, tokens), BF)],
        (routes.T, route_weight.T, residual, out_cot),
    )
    got = lax.all_to_all(
        sent.reshape(experts, SEND_ROWS, lanes), "sp", split_axis=0, concat_axis=0, tiled=True
    )
    (spread,) = call(
        kernel(compact_body, experts, capacity),
        [((blocks, 2 * slots, lanes), BF)],
        (got.reshape(experts * SEND_ROWS, lanes),),
    )
    whole = lax.all_to_all(spread, "tp", 0, 0, tiled=True)
    soft = jax.nn.softplus(-decay_param).reshape(1, channels)
    saved, carry = call(
        state_body,
        [((SAVED, channels, tokens), F32), ((8, tokens), BF)],
        (conv_out, gate_branch, w_recur, w_input, soft),
        flops=20_000_000,
    )
    dxp, acts = call(
        expert_body,
        [((blocks, slots, lanes), BF), ((slots, 3 * hidden), BF)],
        (whole, w_gate[0], w_up[0], w_down[0]),
        flops=10 * slots * hidden * width,
    )
    parts = lax.all_to_all(dxp, "tp", 0, 0, tiled=True)
    grads = expert_grads(whole, acts, width)
    (returned,) = call(
        kernel(owner_sum_body, experts, capacity),
        [((experts * HOME_ROWS, lanes), BF)],
        (parts, carry),
    )
    home = lax.all_to_all(
        returned.reshape(experts, HOME_ROWS, lanes), "sp", split_axis=0, concat_axis=0, tiled=True
    ).reshape(experts * HOME_ROWS, lanes)
    (own,) = call(lift_body, [((blocks, tokens, lanes), BF)], (home, comb, out_cot))
    lifted = lax.all_to_all(own, "tp", 0, 0, tiled=True)
    mix, joined, prods = call(
        join_body,
        [((channels, tokens), BF), ((3, channels, tokens), F32), ((experts, tokens), F32)],
        (me, home, saved),
        flops=20_000_000,
        scalars=1,
        scratch=(pltpu.VMEM((experts, tokens), F32),),
    )
    piece, kept = call(
        last_body,
        [((experts, LAST_ROWS, lanes), BF), ((4, channels, tokens), F32)],
        (lifted, w_out, mix, saved),
    )
    last = lax.all_to_all(piece, "sp", split_axis=0, concat_axis=0, tiled=True)
    g_proj, g_conv, g_branch = call(
        finish_body,
        [((width // experts, channels), F32), ((channels, tokens), F32), ((channels, tokens), F32)],
        (me, last, prods, saved, joined, kept, w_recur, w_input),
        scalars=1,
        scratch=(pltpu.VMEM((experts, tokens), F32),),
    )
    return (grads[0], grads[1], grads[2], g_proj, g_conv, g_branch)


def solution(mesh):
    return jax.shard_map(
        local,
        mesh=mesh,
        in_specs=(
            P("sp", "tp"),
            P("sp", "tp"),
            P("sp", None),
            P("sp", None),
            P("sp", "tp", None),
            P("sp", "tp", None),
            P("sp", "tp", None),
            P("tp", None),
            P("tp", "sp"),
            P("tp", "sp"),
            P("tp", None, None),
            P("tp", None, None),
            P("tp"),
        ),
        out_specs=(
            P("sp", "tp", None),
            P("sp", "tp", None),
            P("sp", "tp", None),
            P("sp", "tp"),
            P("tp", "sp"),
            P("tp", "sp"),
        ),
        check_vma=False,
    )
```

profile of v0, /device:TPU:1, one launch (start us, length us, event | category | flops | bytes accessed | tf_op | source)
XLA Modules:
  0.0 183.2 jit_solution(3803324676212894840)
XLA Ops:
  0.6 0.0 copy-start.13
  0.6 0.7 copy-done.13
  1.4 0.0 copy-start.17
  1.4 0.8 copy-done.17
  2.2 0.0 copy-start.23
  2.2 0.7 copy-done.23
  2.8 0.7 copy-done.24
  3.5 0.5 shard_map.172
  4.1 35.3 %all_to_all.30 = bf16[32,24,128]{2,1,0:T(8,128)(2,1)S(1)} all-to-all(bf16[32,24,128]{2,1,0:T(8,128)(2,1)S(1)} %bitcast.19), channel_id=1, replica_groups=mesh['sp'=32,'tp'=16] {'sp'}, dimensions={0} | all-to-all | bytes 393216 | tf_op jit(solution)/shard_map/all_to_all | solution.py:399
  39.4 0.6 shard_map.173
  40.0 0.0 copy-start.4
  40.0 0.0 copy-start.5
  40.0 0.0 copy-start.6
  40.0 39.4 %all_to_all.31.whole = bf16[16,640,128]{2,1,0:T(8,128)(2,1)S(1)} all-to-all(bf16[16,640,128]{2,1,0:T(8,128)(2,1)S(1)} %shard_map.173), channel_id=1, replica_groups=mesh['sp'=32,'tp'=16] {'tp'}, dimensions={0} | all-to-all | bytes 5242880 | tf_op jit(solution)/shard_map/all_to_all | solution.py:407
  79.4 0.0 copy-done.4
  79.4 0.0 copy-done.5
  79.4 0.0 copy-done.6
  79.4 0.0 copy-start.27
  79.4 0.0 copy-start.18
  79.4 0.0 copy-start.19
  79.4 0.0 copy-start.25
  79.5 0.0 copy-start.26
  79.5 1.3 shard_map.174
  80.8 0.0 copy-start.1
  80.8 1.1 copy-done.1
  81.9 4.5 %all-to-all-start.2 = ((bf16[16,320,128]{2,1,0:T(8,128)(2,1)}), bf16[16,320,128]{2,1,0:T(8,128)(2,1)}, u32[]{:S(2)}, u32[]{:S(2)}) async-start(bf16[16,320,128]{2,1,0:T(8,128)(2,1)} %copy-done.1), calls=%async_computation.2 | async-start | bytes 2621440 | tf_op jit(solution)/shard_map/all_to_all | solution.py:421
  86.4 0.0 copy-done.9
  86.4 0.0 copy-done.27
  86.4 0.0 copy-done.18
  86.4 0.0 copy-done.19
  86.4 0.0 copy-done.25
  86.5 0.0 copy-done.26
  86.5 1.0 shard_map.176
  87.5 16.4 %all-to-all-done.2.refs_0_ = bf16[16,320,128]{2,1,0:T(8,128)(2,1)} async-done(((bf16[16,320,128]{2,1,0:T(8,128)(2,1)}), bf16[16,320,128]{2,1,0:T(8,128)(2,1)}, u32[]{:S(2)}, u32[]{:S(2)}) %all-to-all-start.2) | async-done | bytes 1310752 | tf_op jit(solution)/shard_map/all_to_all | solution.py:421
  103.9 1.8 shard_map.177
  105.7 25.0 %all_to_all.32 = bf16[32,16,128]{2,1,0:T(8,128)(2,1)S(1)} all-to-all(bf16[32,16,128]{2,1,0:T(8,128)(2,1)S(1)} %bitcast.15), channel_id=1, replica_groups=mesh['sp'=32,'tp'=16] {'sp'}, dimensions={0} | all-to-all | bytes 262144 | tf_op jit(solution)/shard_map/all_to_all | solution.py:428
  130.7 0.0 copy-done.14
  130.7 0.2 shard_map.178
  131.0 0.0 copy-start
  131.0 0.8 copy-done
  131.8 0.7 copy-done.2
  132.4 3.6 %all-to-all-start.4 = ((bf16[16,128,128]{2,1,0:T(8,128)(2,1)}), bf16[16,128,128]{2,1,0:T(8,128)(2,1)S(1)}, u32[]{:S(2)}, u32[]{:S(2)}) async-start(bf16[16,128,128]{2,1,0:T(8,128)(2,1)} %copy-done), calls=%async_computation.4 | async-start | bytes 1048576 | tf_op jit(solution)/shard_map/all_to_all | solution.py:432
  136.0 0.0 copy-start.3
  136.0 0.9 copy-done.3
  136.9 0.4 shard_map.179
  137.3 0.0 copy-start.15
  137.4 0.6 copy-done.15
  138.0 0.6 copy-done.21
  138.6 7.5 %all-to-all-done.4.lifted = bf16[16,128,128]{2,1,0:T(8,128)(2,1)S(1)} async-done(((bf16[16,128,128]{2,1,0:T(8,128)(2,1)}), bf16[16,128,128]{2,1,0:T(8,128)(2,1)S(1)}, u32[]{:S(2)}, u32[]{:S(2)}) %all-to-all-start.4) | async-done | bytes 524320 | tf_op jit(solution)/shard_map/all_to_all | solution.py:432
  146.1 0.9 copy-done.8
  147.0 1.2 shard_map.180
  148.2 0.0 copy-start.7
  148.2 0.7 copy-done.7
  149.0 0.7 copy-done.11
  149.6 6.0 %all-to-all-start.5 = ((bf16[32,40,128]{2,1,0:T(8,128)(2,1)}), bf16[32,40,128]{2,1,0:T(8,128)(2,1)S(1)}, u32[]{:S(2)}, u32[]{:S(2)}) async-start(bf16[32,40,128]{2,1,0:T(8,128)(2,1)} %copy-done.7), calls=%async_computation.5 | async-start | bytes 655360 | tf_op jit(solution)/shard_map/all_to_all | solution.py:446
  155.7 0.0 copy-start.10
  155.7 0.9 copy-done.10
  156.6 4.1 %shard_map.175 = (bf16[1,128,2048]{2,1,0:T(8,128)(2,1)}, bf16[1,128,2048]{2,1,0:T(8,128)(2,1)}, bf16[1,128,2048]{2,1,0:T(8,128)(2,1)}) custom-call(bf16[16,640,128]{2,1,0:T(8,128)(2,1)S(1)} %all_to_all.31.whole, bf16[320,384]{1,0:T(8,128)(2,1)S(1)} %copy-done.10), custom_call_target="tpu_custom_call" | custom-call | flops 503316480 | bytes 1572864 | tf_op jit(solution)/shard_map/pallas_call | solution.py:139
  160.7 19.9 %all-to-all-done.5.last = bf16[32,40,128]{2,1,0:T(8,128)(2,1)S(1)} async-done(((bf16[32,40,128]{2,1,0:T(8,128)(2,1)}), bf16[32,40,128]{2,1,0:T(8,128)(2,1)S(1)}, u32[]{:S(2)}, u32[]{:S(2)}) %all-to-all-start.5) | async-done | bytes 327712 | tf_op jit(solution)/shard_map/all_to_all | solution.py:446
  180.6 0.0 copy-done.16
  180.6 0.0 copy-done.12
  180.6 0.7 copy-done.20
  181.4 0.7 copy-done.22
  182.1 1.1 shard_map.181
  (12 shorter events, 0.0 us)
Async XLA Ops:
  0.6 0.8 copy-start.13
  1.4 0.8 copy-start.17
  2.2 0.7 copy-start.23
  2.8 0.7 copy-start.24
  40.0 39.4 %copy-start.4 = (bf16[1,128,2048]{2,1,0:T(8,128)(2,1)S(1)}, bf16[1,128,2048]{2,1,0:T(8,128)(2,1)}, u32[]{:S(2)}) copy-start(bf16[1,128,2048]{2,1,0:T(8,128)(2,1)} %param.17) | copy-start | bytes 1572868
  40.0 39.4 %copy-start.5 = (bf16[1,128,2048]{2,1,0:T(8,128)(2,1)S(1)}, bf16[1,128,2048]{2,1,0:T(8,128)(2,1)}, u32[]{:S(2)}) copy-start(bf16[1,128,2048]{2,1,0:T(8,128)(2,1)} %param.18) | copy-start | bytes 1572868
  40.0 39.4 %copy-start.6 = (bf16[1,128,2048]{2,1,0:T(8,128)(2,1)S(1)}, bf16[1,128,2048]{2,1,0:T(8,128)(2,1)}, u32[]{:S(2)}) copy-start(bf16[1,128,2048]{2,1,0:T(8,128)(2,1)} %param.19) | copy-start | bytes 1572868
  79.4 7.0 %copy-start.27 = (f32[64]{0:T(128)S(1)}, f32[64]{0:T(128)}, u32[]{:S(2)}) copy-start(f32[64]{0:T(128)} %param.25) | copy-start | bytes 772
  79.4 7.0 %copy-start.18 = (bf16[1,64,64]{2,1,0:T(8,128)(2,1)S(1)}, bf16[1,64,64]{2,1,0:T(8,128)(2,1)}, u32[]{:S(2)}) copy-start(bf16[1,64,64]{2,1,0:T(8,128)(2,1)} %w_recur.3) | copy-start | bytes 24580
  79.4 7.0 %copy-start.19 = (bf16[1,64,64]{2,1,0:T(8,128)(2,1)S(1)}, bf16[1,64,64]{2,1,0:T(8,128)(2,1)}, u32[]{:S(2)}) copy-start(bf16[1,64,64]{2,1,0:T(8,128)(2,1)} %w_input.3) | copy-start | bytes 24580
  79.4 7.0 %copy-start.25 = (bf16[64,128]{1,0:T(8,128)(2,1)S(1)}, bf16[64,128]{1,0:T(8,128)(2,1)}, u32[]{:S(2)}) copy-start(bf16[64,128]{1,0:T(8,128)(2,1)} %conv.1) | copy-start | bytes 49156
  79.5 7.0 %copy-start.26 = (bf16[64,128]{1,0:T(8,128)(2,1)S(1)}, bf16[64,128]{1,0:T(8,128)(2,1)}, u32[]{:S(2)}) copy-start(bf16[64,128]{1,0:T(8,128)(2,1)} %branch.1) | copy-start | bytes 49156
  80.8 1.1 copy-start.1
  81.8 4.5 %copy-start.9 = (bf16[320,384]{1,0:T(8,128)(2,1)}, bf16[320,384]{1,0:T(8,128)(2,1)S(1)}, u32[]{:S(2)}) copy-start(bf16[320,384]{1,0:T(8,128)(2,1)S(1)} %get-tuple-element.24.acts) | copy-start | bytes 737284
  81.8 48.9 %copy-start.14 = (bf16[128,128]{1,0:T(8,128)(2,1)S(1)}, bf16[128,128]{1,0:T(8,128)(2,1)}, u32[]{:S(2)}) copy-start(bf16[128,128]{1,0:T(8,128)(2,1)} %cot.1) | copy-start | bytes 98308
  81.9 22.1 %all-to-all-start.2 = ((bf16[16,320,128]{2,1,0:T(8,128)(2,1)}), bf16[16,320,128]{2,1,0:T(8,128)(2,1)}, u32[]{:S(2)}, u32[]{:S(2)}) async-start(bf16[16,320,128]{2,1,0:T(8,128)(2,1)} %copy-done.1), calls=%async_computation.2 | async-start | bytes 2621440 | tf_op jit(solution)/shard_map/all_to_all | solution.py:421
  131.0 0.8 copy-start
  131.8 0.7 copy-start.2
  132.4 13.7 %all-to-all-start.4 = ((bf16[16,128,128]{2,1,0:T(8,128)(2,1)}), bf16[16,128,128]{2,1,0:T(8,128)(2,1)S(1)}, u32[]{:S(2)}, u32[]{:S(2)}) async-start(bf16[16,128,128]{2,1,0:T(8,128)(2,1)} %copy-done), calls=%async_computation.4 | async-start | bytes 1048576 | tf_op jit(solution)/shard_map/all_to_all | solution.py:432
  136.0 0.9 copy-start.3
  137.3 0.6 copy-start.15
  138.0 0.6 copy-start.21
  146.1 1.0 copy-start.8
  148.2 0.7 copy-start.7
  149.0 0.7 copy-start.11
  149.6 31.0 %copy-start.16 = (f32[3,64,128]{2,1,0:T(8,128)S(1)}, f32[3,64,128]{2,1,0:T(8,128)}, u32[]{:S(2)}) copy-start(f32[3,64,128]{2,1,0:T(8,128)} %copy-done.15) | copy-start | bytes 294916
  149.6 31.0 %copy-start.12 = (f32[4,64,128]{2,1,0:T(8,128)S(1)}, f32[4,64,128]{2,1,0:T(8,128)}, u32[]{:S(2)}) copy-start(f32[4,64,128]{2,1,0:T(8,128)} %copy-done.11) | copy-start | bytes 393220
  149.6 31.0 %all-to-all-start.5 = ((bf16[32,40,128]{2,1,0:T(8,128)(2,1)}), bf16[32,40,128]{2,1,0:T(8,128)(2,1)S(1)}, u32[]{:S(2)}, u32[]{:S(2)}) async-start(bf16[32,40,128]{2,1,0:T(8,128)(2,1)} %copy-done.7), calls=%async_computation.5 | async-start | bytes 655360 | tf_op jit(solution)/shard_map/all_to_all | solution.py:446
  155.7 0.9 copy-start.10
  180.6 0.7 copy-start.20
  181.4 0.7 copy-start.22
where the time goes:
time: 184 us; the launch traced here: 183 us
  blocking collectives  99.8 us (54%)
  waiting for transfers between devices  43.9 us (24%)
  starting transfers between devices  14.1 us (8%)
  local copies, waits for them, and re-layouts  12.3 us (7%)
  Pallas kernels  12.2 us (7%)
    all_to_all x1, blocking collectives, local(): whole = lax.all_to_all(spread, 'tp', 0, 0, tiled=True)  39.4 us
    all_to_all x1, blocking collectives, local(): lax.all_to_all(sent.reshape(experts, SEND_ROWS, lanes), 'sp', split_axis=...  35.3 us
    all_to_all x1, blocking collectives, local(): lax.all_to_all(returned.reshape(experts, HOME_ROWS, lanes), 'sp', split_a...  25 us
    all_to_all x1, waiting for transfers between devices, local(): last = lax.all_to_all(piece, 'sp', split_axis=0, concat_axis=0, tiled=True)  19.9 us
    all_to_all x1, waiting for transfers between devices, local(): parts = lax.all_to_all(dxp, 'tp', 0, 0, tiled=True)  16.4 us
    unnamed x56, local copies, waits for them, and re-layouts  12.3 us
    pallas_call x9, Pallas kernels, call(): pl.pallas_call(body, out_shape=[jax.ShapeDtypeStruct(s, d) for s, d in ou...  8.14 us
    all_to_all x1, waiting for transfers between devices, local(): lifted = lax.all_to_all(own, 'tp', 0, 0, tiled=True)  7.49 us
  transfers between devices with their start and end apart: 3, of which 3 were waited for; matrix products, arithmetic and copies ran while one was open for 0% of the time, Pallas kernels for 3%

commit v1 on v0

--- a/solution.py
+++ b/solution.py
@@ -29,15 +29,26 @@
     )
 
 
-def call(body, outs, args, flops=1, bytes_moved=1, scalars=0, scratch=()):
-    specs = [pl.BlockSpec(memory_space=pltpu.SMEM)] * scalars
-    specs += [pl.BlockSpec(memory_space=pltpu.VMEM)] * (len(args) - scalars)
+def call(body, outs, args, flops=1, bytes_moved=1, fetched=0, scratch=(), far=()):
+    specs = [pl.BlockSpec(memory_space=pltpu.HBM)] * fetched
+    specs += [pl.BlockSpec(memory_space=pltpu.VMEM)] * (len(args) - fetched)
+    scratch = [pltpu.VMEM(a.shape, a.dtype) for a in args[:fetched]] + list(scratch)
+    kept = [pltpu.with_memory_space_constraint(a, pltpu.HBM) for a in args[:fetched]]
+    args = kept + list(args[fetched:])
+    if fetched:
+        scratch.append(pltpu.SemaphoreType.DMA((fetched,)))
     return pl.pallas_call(
         body,
-        out_shape=[jax.ShapeDtypeStruct(s, d) for s, d in outs],
+        out_shape=[
+            pltpu.HBM(*out) if k in far else jax.ShapeDtypeStruct(*out)
+            for k, out in enumerate(outs)
+        ],
         in_specs=specs,
-        out_specs=[pl.BlockSpec(memory_space=pltpu.VMEM)] * len(outs),
-        scratch_shapes=list(scratch),
+        out_specs=[
+            pl.BlockSpec(memory_space=pltpu.HBM if k in far else pltpu.VMEM)
+            for k in range(len(outs))
+        ],
+        scratch_shapes=scratch,
         compiler_params=pltpu.CompilerParams(vmem_limit_bytes=24 * 1024 * 1024),
         cost_estimate=pl.CostEstimate(
             flops=flops, bytes_accessed=bytes_moved, transcendentals=0
@@ -45,7 +56,21 @@
     )(*args)
 
 
-def dispatch_body(experts, routes, weight, residual, cot, sent, comb):
+def fetch(sources, targets, sems):
+    copies = [
+        pltpu.make_async_copy(source, target, sems.at[k])
+        for k, (source, target) in enumerate(zip(sources, targets))
+    ]
+    for copy in copies:
+        copy.start()
+    return copies
+
+
+def dispatch_body(experts, *refs):
+    sources, (sent, comb), targets, sems = refs[:4], refs[4:6], refs[6:10], refs[10]
+    for copy in fetch(sources, targets, sems):
+        copy.wait()
+    routes, weight, residual, cot = targets
     tokens = residual.shape[0]
     first, second = routes[0:1, :], routes[1:2, :]
     expert = iota((experts, tokens), 0)
@@ -93,7 +118,11 @@
     return jnp.concatenate([ref[2 * k, lo:hi, :], ref[2 * k + 1, lo:hi, :]], axis=1)
 
 
-def expert_body(whole, w_gate, w_up, w_down, dxp, acts):
+def expert_body(*refs):
+    sources, (whole, w_gate, w_up, w_down) = refs[:5], refs[5:9]
+    dxp, far_acts, saved, carry = refs[9:13]
+    targets, acts, acts_sem, sems = refs[13:18], refs[18], refs[19], refs[20]
+    copies = fetch(sources, targets, sems)
     slots = whole.shape[1] // 2
     blocks = whole.shape[0]
     hidden = w_gate.shape[0]
@@ -114,12 +143,18 @@
     cots = jnp.concatenate([gate_cot, up_cot], axis=1)
     acts[:, : 2 * hidden] = cots
     acts[:, 2 * hidden :] = act
+    write = pltpu.make_async_copy(acts, far_acts, acts_sem)
+    write.start()
     for k in range(blocks // 2):
         cols = slice(256 * k, 256 * (k + 1))
         both = jnp.concatenate([w_gate[:, cols], w_up[:, cols]], axis=0)
         part = dot(cots, both).astype(BF)
         dxp[2 * k] = part[:, :128]
         dxp[2 * k + 1] = part[:, 128:]
+    for copy in copies:
+        copy.wait()
+    state_body(*targets, saved, carry)
+    write.wait()
 
 
 def grads_body(whole, acts, g_gate, g_up, g_down):
@@ -166,11 +201,12 @@
     out[...] = (dot(pick, total) + dot(extra, carry[...])).astype(BF)
 
 
-def lift_body(home, comb, cot, out):
+def lift_body(home, comb, cot, saved, out, mix, ends, adds):
     grad = dot(comb[...], home[...], 0, 0)
     lifted = (cot[...].astype(F32) + grad).astype(BF)
     for j in range(out.shape[0]):
         out[j] = lifted
+    join_body(home, saved, mix, ends, adds)
 
 
 def shift_in(x, d, fill, lane):
@@ -229,14 +265,24 @@
     return total
 
 
-SAVED = 11
-
-
-def state_body(conv, branch, w_recur, w_input, soft, saved, carry):
+SAVED = 12
+
+
+def soft_plus(x):
+    small = jnp.exp(-jnp.abs(x))
+    z = small / (2.0 + small)
+    square = z * z
+    series = jnp.full_like(z, 1.0 / 19.0)
+    for odd in (17, 15, 13, 11, 9, 7, 5, 3, 1):
+        series = series * square + 1.0 / odd
+    return jnp.maximum(x, 0.0) + 2.0 * z * series
+
+
+def state_body(conv, branch, w_recur, w_input, decay_param, saved, carry):
     channels, tokens = conv.shape
     lane = iota((channels, tokens), 1)
     eye = iota((channels, channels), 0) == iota((channels, channels), 1)
-    softness = jnp.sum(jnp.where(eye, soft[...], 0.0), axis=1, keepdims=True)
+    softness = jnp.sum(jnp.where(eye, soft_plus(-decay_param[...]), 0.0), axis=1, keepdims=True)
     values = conv[...].astype(F32)
     sig_r = jax.nn.sigmoid(dot(w_recur[0], conv[...], 0, 0))
     sig_a = jax.nn.sigmoid(dot(w_input[0], conv[...], 0, 0))
@@ -261,6 +307,7 @@
     saved[8] = -(decay / root) * sig_a * values
     saved[9] = root * values * sig_a * (1.0 - sig_a)
     saved[10] = direct
+    saved[11] = jnp.concatenate([w_recur[0], w_input[0]], axis=1).astype(F32)
     rows = in_three(ends_row(up_prod, down_prod, lane)) + in_three(
         ends_row(up_state, down_state, lane)
     )
@@ -271,28 +318,29 @@
     carry[...] = total.astype(BF)
 
 
-def join_body(me, home, saved, mix, joined, prods, adds):
-    devices = prods.shape[0]
+def joined_states(saved, state_in, state_back):
+    return saved[2] + saved[1] * state_in, saved[4] + saved[3] * state_back
+
+
+def join_body(home, saved, mix, ends, adds):
     channels, tokens = mix.shape
+    devices = adds.shape[0]
     rows = home.shape[0]
     lane = iota((channels, tokens), 1)
     offset = iota((devices, rows), 1) - HOME_ROWS * iota((devices, rows), 0)
     base = HOME_ROWS - 6
     prod_rows = ((offset >= base) & (offset < base + 3)).astype(F32).astype(BF)
     add_rows = ((offset >= base + 3) & (offset < base + 6)).astype(F32).astype(BF)
+    prods = ends.at[channels:, :]
     prods[...] = dot(prod_rows, home[...])
     adds[...] = dot(add_rows, home[...])
-    state_in, state_back = to_columns(fold(me[0], prods, adds, channels), lane)
-    fwd = saved[2] + saved[1] * state_in
-    bwd = saved[4] + saved[3] * state_back
-    total = fwd + bwd
-    mix[...] = (saved[5] * total).astype(BF)
-    joined[0] = jnp.where(lane == 0, state_in, pltpu.roll(fwd, 1, 1))
-    joined[1] = jnp.where(lane == tokens - 1, state_back, pltpu.roll(bwd, tokens - 1, 1))
-    joined[2] = total * saved[6]
-
-
-def last_body(lifted, w_out, mix, saved, out, kept):
+    state_in, state_back = to_columns(fold(lax.axis_index("sp"), prods, adds, channels), lane)
+    ends[:channels, :] = jnp.where(lane < channels, state_in, state_back)
+    fwd, bwd = joined_states(saved, state_in, state_back)
+    mix[...] = (saved[5] * (fwd + bwd)).astype(BF)
+
+
+def last_body(lifted, w_out, mix, saved, far_out, kept, out, sems):
     blocks, tokens, _ = lifted.shape
     channels = mix.shape[0]
     half = channels // 2
@@ -310,6 +358,8 @@
             spot = 4 * k + 2 * q
             out[spot, :half, :] = jnp.where(left, top, pltpu.roll(bottom, 64, 1)).astype(BF)
             out[spot + 1, :half, :] = jnp.where(left, pltpu.roll(top, 64, 1), bottom).astype(BF)
+    first = pltpu.make_async_copy(out.at[:, :half, :], far_out.at[:, :half, :], sems.at[0])
+    first.start()
     decay = saved[0]
     cot = mix_cot * saved[5]
     weighted = decay * cot
@@ -327,38 +377,45 @@
     total = total.astype(BF)
     for s in range(out.shape[0]):
         out[s, half:, :] = total
-
-
-def finish_body(me, last, prods, saved, joined, kept, w_recur, w_input, g_proj, g_conv, g_branch, adds):
-    devices = prods.shape[0]
+    second = pltpu.make_async_copy(out.at[:, half:, :], far_out.at[:, half:, :], sems.at[1])
+    second.start()
+    first.wait()
+    second.wait()
+
+
+def finish_body(last, ends, saved, kept, g_proj, g_conv, g_branch, adds):
+    devices = adds.shape[0]
     channels, tokens = g_conv.shape
+    prods = ends.at[channels:, :]
     half = channels // 2
     lane = iota((channels, tokens), 1)
     total = last[0, :half, :].astype(F32)
-    carry = jnp.zeros((8, tokens), F32)
     for s in range(devices):
         if s:
             total = total + last[s, :half, :].astype(F32)
         adds[s : s + 1, :] = jnp.sum(last[s, half:, :].astype(F32), axis=0, keepdims=True)
     turned = total.T
     g_proj[...] = jnp.concatenate([turned[:64], turned[64:]], axis=1)
-    adj_in, adj_back = to_columns(fold(me[0], prods, adds, channels), lane)
+    adj_in, adj_back = to_columns(fold(lax.axis_index("sp"), prods, adds, channels), lane)
+    state_in, state_back = ends[:channels, :1], ends[:channels, tokens - 1 :]
+    fwd, bwd = joined_states(saved, state_in, state_back)
+    before = jnp.where(lane == 0, state_in, pltpu.roll(fwd, 1, 1))
+    after = jnp.where(lane == tokens - 1, state_back, pltpu.roll(bwd, tokens - 1, 1))
     cot = kept[1]
     up = kept[2] + saved[1] * adj_in
     down = kept[3] + saved[3] * adj_back
     past = cot + jnp.where(lane == 0, adj_in, pltpu.roll(up, 1, 1))
     future = cot + jnp.where(lane == tokens - 1, adj_back, pltpu.roll(down, tokens - 1, 1))
     drive_cot = past + future
-    decay_cot = future * joined[0] + past * joined[1] + drive_cot * saved[8]
+    decay_cot = future * before + past * after + drive_cot * saved[8]
     recur_cot = decay_cot * saved[7]
     admit_cot = drive_cot * saved[9]
     exact = lax.Precision.HIGHEST
     g_conv[...] = (
         drive_cot * saved[10]
-        + dot(w_recur[0].astype(F32), recur_cot, 1, 0, exact)
-        + dot(w_input[0].astype(F32), admit_cot, 1, 0, exact)
-    )
-    g_branch[...] = kept[0] * joined[2]
+        + dot(saved[11], jnp.concatenate([recur_cot, admit_cot], axis=0), 1, 0, exact)
+    )
+    g_branch[...] = kept[0] * (fwd + bwd) * saved[6]
 
 
 def local(
@@ -378,7 +435,6 @@
 ):
     experts = lax.axis_size("sp")
     blocks = lax.axis_size("tp")
-    me = lax.axis_index("sp").reshape(1).astype(I32)
     tokens, lanes = residual.shape
     capacity = 2 * tokens // experts + 2
     slots = experts * capacity
@@ -395,6 +451,7 @@
         kernel(dispatch_body, experts),
         [((experts * SEND_ROWS, lanes), BF), ((experts * HOME_ROWS, tokens), BF)],
         (routes.T, route_weight.T, residual, out_cot),
+        fetched=4,
     )
     got = lax.all_to_all(
         sent.reshape(experts, SEND_ROWS, lanes), "sp", split_axis=0, concat_axis=0, tiled=True
@@ -405,21 +462,31 @@
         (got.reshape(experts * SEND_ROWS, lanes),),
     )
     whole = lax.all_to_all(spread, "tp", 0, 0, tiled=True)
-    soft = jax.nn.softplus(-decay_param).reshape(1, channels)
-    saved, carry = call(
-        state_body,
-        [((SAVED, channels, tokens), F32), ((8, tokens), BF)],
-        (conv_out, gate_branch, w_recur, w_input, soft),
-        flops=20_000_000,
-    )
-    dxp, acts = call(
+    dxp, acts, saved, carry = call(
         expert_body,
-        [((blocks, slots, lanes), BF), ((slots, 3 * hidden), BF)],
-        (whole, w_gate[0], w_up[0], w_down[0]),
+        [
+            ((blocks, slots, lanes), BF),
+            ((slots, 3 * hidden), BF),
+            ((SAVED, channels, tokens), F32),
+            ((8, tokens), BF),
+        ],
+        (
+            conv_out,
+            gate_branch,
+            w_recur,
+            w_input,
+            decay_param.reshape(1, channels),
+            whole,
+            w_gate[0],
+            w_up[0],
+            w_down[0],
+        ),
+        fetched=5,
+        scratch=(pltpu.VMEM((slots, 3 * hidden), BF), pltpu.SemaphoreType.DMA),
+        far=(1,),
         flops=10 * slots * hidden * width,
     )
     parts = lax.all_to_all(dxp, "tp", 0, 0, tiled=True)
-    grads = expert_grads(whole, acts, width)
     (returned,) = call(
         kernel(owner_sum_body, experts, capacity),
         [((experts * HOME_ROWS, lanes), BF)],
@@ -428,27 +495,31 @@
     home = lax.all_to_all(
         returned.reshape(experts, HOME_ROWS, lanes), "sp", split_axis=0, concat_axis=0, tiled=True
     ).reshape(experts * HOME_ROWS, lanes)
-    (own,) = call(lift_body, [((blocks, tokens, lanes), BF)], (home, comb, out_cot))
+    own, mix, ends = call(
+        lift_body,
+        [
+            ((blocks, tokens, lanes), BF),
+            ((channels, tokens), BF),
+            ((channels + experts, tokens), F32),
+        ],
+        (home, comb, out_cot, saved),
+        scratch=(pltpu.VMEM((experts, tokens), F32),),
+    )
     lifted = lax.all_to_all(own, "tp", 0, 0, tiled=True)
-    mix, joined, prods = call(
-        join_body,
-        [((channels, tokens), BF), ((3, channels, tokens), F32), ((experts, tokens), F32)],
-        (me, home, saved),
-        flops=20_000_000,
-        scalars=1,
-        scratch=(pltpu.VMEM((experts, tokens), F32),),
-    )
     piece, kept = call(
         last_body,
         [((experts, LAST_ROWS, lanes), BF), ((4, channels, tokens), F32)],
         (lifted, w_out, mix, saved),
-    )
+        scratch=(pltpu.VMEM((experts, LAST_ROWS, lanes), BF), pltpu.SemaphoreType.DMA((2,))),
+        far=(0,),
+    )
+    piece, acts = lax.optimization_barrier((piece, acts))
+    grads = expert_grads(whole, acts, width)
     last = lax.all_to_all(piece, "sp", split_axis=0, concat_axis=0, tiled=True)
     g_proj, g_conv, g_branch = call(
         finish_body,
         [((width // experts, channels), F32), ((channels, tokens), F32), ((channels, tokens), F32)],
-        (me, last, prods, saved, joined, kept, w_recur, w_input),
-        scalars=1,
+        (last, ends, saved, kept),
         scratch=(pltpu.VMEM((experts, tokens), F32),),
     )
     return (grads[0], grads[1], grads[2], g_proj, g_conv, g_branch)

time: 184 us -> 172 us (0.935)
  blocking collectives: 99.8 us -> 131 us
  waiting for transfers between devices: 43.9 us -> 19.9 us
  local copies, waits for them, and re-layouts: 12.3 us -> 0.97 us
  starting transfers between devices: 14.1 us -> 6.07 us
    all_to_all x0 -> x2, blocking collectives: none -> 32.9 us  [the longest x1 20.3 us: local(): parts = lax.all_to_all(dxp, 'tp', 0, 0, tiled=True)]
    all_to_all x2 -> x0, waiting for transfers between devices: 23.9 us -> none  [the longest x1 16.4 us: local(): parts = lax.all_to_all(dxp, 'tp', 0, 0, tiled=True)]
    unnamed x56 -> x12, local copies, waits for them, and re-layouts: 12.3 us -> 0.97 us
    all_to_all x2 -> x0, starting transfers between devices: 8.1 us -> none  [the longest x1 4.53 us: local(): parts = lax.all_to_all(dxp, 'tp', 0, 0, tiled=True)]
    pallas_call x9 -> x7, Pallas kernels: 8.14 us -> 8.35 us  [call(): pl.pallas_call(body, out_shape=[pltpu.HBM(*out) if k in far else jax.Shap...]
  transfers between devices with their start and end apart: 3 -> 1, of which waited for: 3 -> 1; matrix products, arithmetic and copies ran while one was open for 0% -> 0% of each run, Pallas kernels for 3% -> 2%
where the time goes in v1:
time: 172 us; the launch traced here: 171 us
  blocking collectives  131 us (76%)
  waiting for transfers between devices  19.9 us (12%)
  Pallas kernels  12.4 us (7%)
  starting transfers between devices  6.07 us (4%)
    all_to_all x1, blocking collectives, local(): whole = lax.all_to_all(spread, 'tp', 0, 0, tiled=True)  39.4 us
    all_to_all x1, blocking collectives, local(): lax.all_to_all(sent.reshape(experts, SEND_ROWS, lanes), 'sp', split_axis=...  35.3 us
    all_to_all x1, blocking collectives, local(): lax.all_to_all(returned.reshape(experts, HOME_ROWS, lanes), 'sp', split_a...  23.5 us
    all_to_all x1, blocking collectives, local(): parts = lax.all_to_all(dxp, 'tp', 0, 0, tiled=True)  20.3 us
    all_to_all x1, waiting for transfers between devices, local(): last = lax.all_to_all(piece, 'sp', split_axis=0, concat_axis=0, tiled=True)  19.9 us
    all_to_all x1, blocking collectives, local(): lifted = lax.all_to_all(own, 'tp', 0, 0, tiled=True)  12.6 us
    pallas_call x7, Pallas kernels, call(): pl.pallas_call(body, out_shape=[pltpu.HBM(*out) if k in far else jax.Shap...  8.35 us
    all_to_all x1, starting transfers between devices, local(): last = lax.all_to_all(piece, 'sp', split_axis=0, concat_axis=0, tiled=True)  6.07 us
  transfers between devices with their start and end apart: 1, of which 1 were waited for; matrix products, arithmetic and copies ran while one was open for 0% of the time, Pallas kernels for 2%

profile of v1, /device:TPU:1, one launch (start us, length us, event | category | flops | bytes accessed | tf_op | source)
XLA Modules:
  0.0 171.3 jit_solution(14441980187857377574)
XLA Ops:
  0.6 1.4 shard_map.172
  2.0 35.3 %all_to_all.30 = bf16[32,24,128]{2,1,0:T(8,128)(2,1)S(1)} all-to-all(bf16[32,24,128]{2,1,0:T(8,128)(2,1)S(1)} %bitcast.16), channel_id=1, replica_groups=mesh['sp'=32,'tp'=16] {'sp'}, dimensions={0} | all-to-all | bytes 393216 | tf_op jit(solution)/shard_map/all_to_all | solution.py:456
  37.3 0.6 shard_map.173
  37.9 0.0 copy-start
  37.9 0.0 copy-start.1
  37.9 0.0 copy-start.2
  37.9 39.4 %all_to_all.31.refs_5_.whole = bf16[16,640,128]{2,1,0:T(8,128)(2,1)S(1)} all-to-all(bf16[16,640,128]{2,1,0:T(8,128)(2,1)S(1)} %shard_map.173), channel_id=1, replica_groups=mesh['sp'=32,'tp'=16] {'tp'}, dimensions={0} | all-to-all | bytes 5242880 | tf_op jit(solution)/shard_map/all_to_all | solution.py:464
  77.3 0.0 copy-done
  77.3 0.0 copy-done.1
  77.3 0.0 copy-done.2
  77.4 2.5 %shard_map.174 = (bf16[16,320,128]{2,1,0:T(8,128)(2,1)S(1)}, bf16[320,384]{1,0:T(8,128)(2,1)}, f32[12,64,128]{2,1,0:T(8,128)S(1)}, bf16[8,128]{1,0:T(8,128)(2,1)S(1)}) custom-call(bf16[64,128]{1,0:T(8,128)(2,1)} %refs_0_.1, bf16[64,128]{1,0:T(8,128)(2,1)} %refs_1_.1, bf16[1,64,64]{2,1,0:T(8,128)(2,1)} %refs_2_.3, bf16[1,64,64]{2,1,0:T(8,128)(2,1)} %refs_3_.3, ...), custom_call_target="tpu_custom_call" | custom-call | flops 838860800 | bytes 1 | tf_op jit(solution)/shard_map/pallas_call | solution.py:40
  79.9 0.0 copy-start.5
  79.9 0.0 copy-start.3
  79.9 20.3 %all_to_all.32.refs_0_ = bf16[16,320,128]{2,1,0:T(8,128)(2,1)S(1)} all-to-all(bf16[16,320,128]{2,1,0:T(8,128)(2,1)S(1)} %get-tuple-element.26), channel_id=1, replica_groups=mesh['sp'=32,'tp'=16] {'tp'}, dimensions={0} | all-to-all | bytes 2621440 | tf_op jit(solution)/shard_map/all_to_all | solution.py:489
  100.2 0.5 shard_map.175
  100.7 23.5 %all_to_all.33 = bf16[32,16,128]{2,1,0:T(8,128)(2,1)S(1)} all-to-all(bf16[32,16,128]{2,1,0:T(8,128)(2,1)S(1)} %bitcast.15), channel_id=1, replica_groups=mesh['sp'=32,'tp'=16] {'sp'}, dimensions={0} | all-to-all | bytes 262144 | tf_op jit(solution)/shard_map/all_to_all | solution.py:495
  124.2 0.0 copy-done.5
  124.2 0.5 shard_map.176
  124.6 12.6 %all_to_all.34.lifted = bf16[16,128,128]{2,1,0:T(8,128)(2,1)S(1)} all-to-all(bf16[16,128,128]{2,1,0:T(8,128)(2,1)S(1)} %get-tuple-element.30), channel_id=1, replica_groups=mesh['sp'=32,'tp'=16] {'tp'}, dimensions={0} | all-to-all | bytes 1048576 | tf_op jit(solution)/shard_map/all_to_all | solution.py:508
  137.2 0.0 copy-done.3
  137.2 1.9 %shard_map.177 = (bf16[32,40,128]{2,1,0:T(8,128)(2,1)}, f32[4,64,128]{2,1,0:T(8,128)S(1)}) custom-call(bf16[16,128,128]{2,1,0:T(8,128)(2,1)S(1)} %all_to_all.34.lifted, bf16[64,2048]{1,0:T(8,128)(2,1)S(1)} %copy-done.3, bf16[64,128]{1,0:T(8,128)(2,1)S(1)} %get-tuple-element.31.mix, f32[12,64,128]{2,1,0:T(8,128)S(1)} %get-tuple-element.29.saved), custom_call_target="tpu_custom_call" | custom-call | flops 1 | bytes 1 | tf_op jit(solution)/shard_map/pallas_call | solution.py:40
  139.1 6.1 %all-to-all-start.5 = ((bf16[32,40,128]{2,1,0:T(8,128)(2,1)}), bf16[32,40,128]{2,1,0:T(8,128)(2,1)S(1)}, u32[]{:S(2)}, u32[]{:S(2)}) async-start(bf16[32,40,128]{2,1,0:T(8,128)(2,1)} %get-tuple-element.38), calls=%async_computation.5 | async-start | bytes 655360 | tf_op jit(solution)/shard_map/all_to_all | solution.py:518
  145.2 0.0 copy-start.4
  145.2 0.9 copy-done.4
  146.1 4.1 %shard_map.178 = (bf16[1,128,2048]{2,1,0:T(8,128)(2,1)}, bf16[1,128,2048]{2,1,0:T(8,128)(2,1)}, bf16[1,128,2048]{2,1,0:T(8,128)(2,1)}) custom-call(bf16[16,640,128]{2,1,0:T(8,128)(2,1)S(1)} %all_to_all.31.refs_5_.whole, bf16[320,384]{1,0:T(8,128)(2,1)S(1)} %copy-done.4), custom_call_target="tpu_custom_call" | custom-call | flops 503316480 | bytes 1572864 | tf_op jit(solution)/shard_map/pallas_call | solution.py:174
  150.2 19.9 %all-to-all-done.5.last = bf16[32,40,128]{2,1,0:T(8,128)(2,1)S(1)} async-done(((bf16[32,40,128]{2,1,0:T(8,128)(2,1)}), bf16[32,40,128]{2,1,0:T(8,128)(2,1)S(1)}, u32[]{:S(2)}, u32[]{:S(2)}) %all-to-all-start.5) | async-done | bytes 327712 | tf_op jit(solution)/shard_map/all_to_all | solution.py:518
  170.2 1.1 shard_map.179
Async XLA Ops:
  37.9 39.4 %copy-start = (bf16[1,128,2048]{2,1,0:T(8,128)(2,1)S(1)}, bf16[1,128,2048]{2,1,0:T(8,128)(2,1)}, u32[]{:S(2)}) copy-start(bf16[1,128,2048]{2,1,0:T(8,128)(2,1)} %param.17) | copy-start | bytes 1572868
  37.9 39.4 %copy-start.1 = (bf16[1,128,2048]{2,1,0:T(8,128)(2,1)S(1)}, bf16[1,128,2048]{2,1,0:T(8,128)(2,1)}, u32[]{:S(2)}) copy-start(bf16[1,128,2048]{2,1,0:T(8,128)(2,1)} %param.18) | copy-start | bytes 1572868
  37.9 39.4 %copy-start.2 = (bf16[1,128,2048]{2,1,0:T(8,128)(2,1)S(1)}, bf16[1,128,2048]{2,1,0:T(8,128)(2,1)}, u32[]{:S(2)}) copy-start(bf16[1,128,2048]{2,1,0:T(8,128)(2,1)} %param.19) | copy-start | bytes 1572868
  79.9 44.3 %copy-start.5 = (bf16[128,128]{1,0:T(8,128)(2,1)S(1)}, bf16[128,128]{1,0:T(8,128)(2,1)}, u32[]{:S(2)}) copy-start(bf16[128,128]{1,0:T(8,128)(2,1)} %cot.1) | copy-start | bytes 98308
  79.9 57.3 %copy-start.3 = (bf16[64,2048]{1,0:T(8,128)(2,1)S(1)}, bf16[64,2048]{1,0:T(8,128)(2,1)}, u32[]{:S(2)}) copy-start(bf16[64,2048]{1,0:T(8,128)(2,1)} %w_out.1) | copy-start | bytes 786436
  139.1 31.1 %all-to-all-start.5 = ((bf16[32,40,128]{2,1,0:T(8,128)(2,1)}), bf16[32,40,128]{2,1,0:T(8,128)(2,1)S(1)}, u32[]{:S(2)}, u32[]{:S(2)}) async-start(bf16[32,40,128]{2,1,0:T(8,128)(2,1)} %get-tuple-element.38), calls=%async_computation.5 | async-start | bytes 655360 | tf_op jit(solution)/shard_map/all_to_all | solution.py:518
  145.2 0.9 copy-start.4

commit v2 on v1

--- a/solution.py
+++ b/solution.py
@@ -14,9 +14,8 @@
 F32 = jnp.float32
 I32 = jnp.int32
 
-SEND_ROWS = 24
 HOME_ROWS = 16
-LAST_ROWS = 40
+GROUP = 4
 
 
 def iota(shape, dim):
@@ -83,33 +82,47 @@
     back = iota((experts * HOME_ROWS, tokens), 0)
     at_home = (back == first * HOME_ROWS + slot0) | (back == second * HOME_ROWS + slot1)
     comb[...] = at_home.astype(F32).astype(BF)
-    row = iota((experts * SEND_ROWS, tokens), 0)
-    place0 = first * SEND_ROWS + slot0
-    place1 = second * SEND_ROWS + slot1
-    in_rows = ((row == place0) | (row == place1)).astype(F32).astype(BF)
-    capacity = SEND_ROWS // 2 - 2
-    cot0 = row == place0 + capacity
-    cot1 = row == place1 + capacity
-    factor = jnp.sum(
-        jnp.where(cot0, weight[0:1, :], 0.0) + jnp.where(cot1, weight[1:2, :], 0.0),
-        axis=1,
-        keepdims=True,
-    )
-    cot_rows = (cot0 | cot1).astype(F32).astype(BF)
-    rows = dot(in_rows, residual[...]) + factor * dot(cot_rows, cot[...])
-    sent[...] = rows.astype(BF)
+    count = sent.shape[2] // tokens
+    capacity = GROUP * count // 2
+    row = iota((experts * GROUP, tokens), 0)
+    place0 = first * 2 * capacity + slot0
+    place1 = second * 2 * capacity + slot1
+    spot = (row & (GROUP - 1)) + (row >> 2) * 2 * capacity
+    for k in range(count):
+        here = spot + GROUP * k
+        in_rows = ((here == place0) | (here == place1)).astype(F32).astype(BF)
+        cot0 = here == place0 + capacity
+        cot1 = here == place1 + capacity
+        factor = jnp.sum(
+            jnp.where(cot0, weight[0:1, :], 0.0) + jnp.where(cot1, weight[1:2, :], 0.0),
+            axis=1,
+            keepdims=True,
+        )
+        cot_rows = (cot0 | cot1).astype(F32).astype(BF)
+        rows = dot(in_rows, residual[...]) + factor * dot(cot_rows, cot[...])
+        for e in range(experts):
+            sent[e, :, tokens * k : tokens * (k + 1)] = rows[GROUP * e : GROUP * (e + 1)].astype(BF)
 
 
 def compact_body(experts, capacity, got, out):
     slots = experts * capacity
-    total = got.shape[0]
+    lanes = out.shape[2]
+    count = got.shape[2] // lanes
+    blocks = [
+        jnp.concatenate(
+            [got[e, :, lanes * k : lanes * (k + 1)].astype(F32) for e in range(experts)], axis=0
+        )
+        for k in range(count)
+    ]
     row = iota((2 * slots, 1), 0)
     half = (row >= slots).astype(I32)
     rest = row - half * slots
     source = jnp.floor((rest.astype(F32) + 0.5) * (1.0 / capacity)).astype(I32)
-    target = source * SEND_ROWS + half * capacity + (rest - source * capacity)
+    inner = half * capacity + (rest - source * capacity)
+    target = (inner >> 2) * experts * GROUP + source * GROUP + (inner & (GROUP - 1))
+    total = count * experts * GROUP
     pick = (iota((2 * slots, total), 1) == target).astype(F32).astype(BF)
-    rows = dot(pick, got[...]).astype(BF)
+    rows = dot(pick, jnp.concatenate(blocks, axis=0).astype(BF)).astype(BF)
     for j in range(out.shape[0]):
         out[j] = rows
 
@@ -340,7 +353,13 @@
     mix[...] = (saved[5] * (fwd + bwd)).astype(BF)
 
 
-def last_body(lifted, w_out, mix, saved, far_out, kept, out, sems):
+def in_groups(out, spot, rows):
+    width = rows.shape[1]
+    for k in range(rows.shape[0] // GROUP):
+        out[spot, :, width * k : width * (k + 1)] = rows[GROUP * k : GROUP * (k + 1)].astype(BF)
+
+
+def last_body(lifted, w_out, mix, saved, ends, far_out, far_kept, out, kept, sems):
     blocks, tokens, _ = lifted.shape
     channels = mix.shape[0]
     half = channels // 2
@@ -356,54 +375,63 @@
             part = proj[:, 128 * q : 128 * (q + 1)]
             top, bottom = part[:half], part[half:]
             spot = 4 * k + 2 * q
-            out[spot, :half, :] = jnp.where(left, top, pltpu.roll(bottom, 64, 1)).astype(BF)
-            out[spot + 1, :half, :] = jnp.where(left, pltpu.roll(top, 64, 1), bottom).astype(BF)
-    first = pltpu.make_async_copy(out.at[:, :half, :], far_out.at[:, :half, :], sems.at[0])
+            in_groups(out, spot, jnp.where(left, top, pltpu.roll(bottom, 64, 1)))
+            in_groups(out, spot + 1, jnp.where(left, pltpu.roll(top, 64, 1), bottom))
+    cut = half // GROUP * 128
+    first = pltpu.make_async_copy(out.at[:, :, :cut], far_out.at[:, :, :cut], sems.at[0])
     first.start()
     decay = saved[0]
     cot = mix_cot * saved[5]
     weighted = decay * cot
     _, up = scan(decay, weighted, lane, shift_in)
     _, down = scan(decay, weighted, lane, shift_out)
-    kept[0] = mix_cot
-    kept[1] = cot
-    kept[2] = up
-    kept[3] = down
+    kept[:channels] = mix_cot
+    kept[channels : 2 * channels] = cot
+    kept[2 * channels : 3 * channels] = up
+    kept[3 * channels : 4 * channels] = down
+    kept[4 * channels :] = ends[...]
+    third = pltpu.make_async_copy(kept, far_kept, sems.at[2])
+    third.start()
     rows = in_three(ends_row(up, down, lane))
     place = iota((8, tokens), 0)
     total = jnp.zeros((8, tokens), F32)
     for k, row in enumerate(rows):
         total = jnp.where(place == k, row.astype(F32), total)
-    total = total.astype(BF)
+    total = total[:GROUP].astype(BF)
     for s in range(out.shape[0]):
-        out[s, half:, :] = total
-    second = pltpu.make_async_copy(out.at[:, half:, :], far_out.at[:, half:, :], sems.at[1])
+        out[s, :, cut:] = total
+    second = pltpu.make_async_copy(out.at[:, :, cut:], far_out.at[:, :, cut:], sems.at[1])
     second.start()
     first.wait()
+    third.wait()
     second.wait()
 
 
-def finish_body(last, ends, saved, kept, g_proj, g_conv, g_branch, adds):
+def finish_body(far_kept, last, saved, g_proj, g_conv, g_branch, kept, adds, sems):
+    (copy,) = fetch((far_kept,), (kept,), sems)
     devices = adds.shape[0]
     channels, tokens = g_conv.shape
-    prods = ends.at[channels:, :]
+    ends = kept.at[4 * channels :, :]
+    prods = kept.at[5 * channels :, :]
     half = channels // 2
     lane = iota((channels, tokens), 1)
-    total = last[0, :half, :].astype(F32)
+    cut = half // GROUP * 128
+    total = last[0, :, :cut].astype(F32)
     for s in range(devices):
         if s:
-            total = total + last[s, :half, :].astype(F32)
-        adds[s : s + 1, :] = jnp.sum(last[s, half:, :].astype(F32), axis=0, keepdims=True)
-    turned = total.T
+            total = total + last[s, :, :cut].astype(F32)
+        adds[s : s + 1, :] = jnp.sum(last[s, :, cut:].astype(F32), axis=0, keepdims=True)
+    turned = jnp.concatenate([total[:, k : k + 128] for k in range(0, cut, 128)], axis=0).T
     g_proj[...] = jnp.concatenate([turned[:64], turned[64:]], axis=1)
+    copy.wait()
     adj_in, adj_back = to_columns(fold(lax.axis_index("sp"), prods, adds, channels), lane)
     state_in, state_back = ends[:channels, :1], ends[:channels, tokens - 1 :]
     fwd, bwd = joined_states(saved, state_in, state_back)
     before = jnp.where(lane == 0, state_in, pltpu.roll(fwd, 1, 1))
     after = jnp.where(lane == tokens - 1, state_back, pltpu.roll(bwd, tokens - 1, 1))
-    cot = kept[1]
-    up = kept[2] + saved[1] * adj_in
-    down = kept[3] + saved[3] * adj_back
+    cot = kept[channels : 2 * channels]
+    up = kept[2 * channels : 3 * channels] + saved[1] * adj_in
+    down = kept[3 * channels : 4 * channels] + saved[3] * adj_back
     past = cot + jnp.where(lane == 0, adj_in, pltpu.roll(up, 1, 1))
     future = cot + jnp.where(lane == tokens - 1, adj_back, pltpu.roll(down, tokens - 1, 1))
     drive_cot = past + future
@@ -415,7 +443,7 @@
         drive_cot * saved[10]
         + dot(saved[11], jnp.concatenate([recur_cot, admit_cot], axis=0), 1, 0, exact)
     )
-    g_branch[...] = kept[0] * (fwd + bwd) * saved[6]
+    g_branch[...] = kept[:channels] * (fwd + bwd) * saved[6]
 
 
 def local(
@@ -449,17 +477,18 @@
 
     sent, comb = call(
         kernel(dispatch_body, experts),
-        [((experts * SEND_ROWS, lanes), BF), ((experts * HOME_ROWS, tokens), BF)],
+        [
+            ((experts, GROUP, 2 * capacity // GROUP * lanes), BF),
+            ((experts * HOME_ROWS, tokens), BF),
+        ],
         (routes.T, route_weight.T, residual, out_cot),
         fetched=4,
     )
-    got = lax.all_to_all(
-        sent.reshape(experts, SEND_ROWS, lanes), "sp", split_axis=0, concat_axis=0, tiled=True
-    )
+    got = lax.all_to_all(sent, "sp", split_axis=0, concat_axis=0, tiled=True)
     (spread,) = call(
         kernel(compact_body, experts, capacity),
         [((blocks, 2 * slots, lanes), BF)],
-        (got.reshape(experts * SEND_ROWS, lanes),),
+        (got,),
     )
     whole = lax.all_to_all(spread, "tp", 0, 0, tiled=True)
     dxp, acts, saved, carry = call(
@@ -506,12 +535,17 @@
         scratch=(pltpu.VMEM((experts, tokens), F32),),
     )
     lifted = lax.all_to_all(own, "tp", 0, 0, tiled=True)
+    last_width = (channels // 2 // GROUP + 1) * lanes
     piece, kept = call(
         last_body,
-        [((experts, LAST_ROWS, lanes), BF), ((4, channels, tokens), F32)],
-        (lifted, w_out, mix, saved),
-        scratch=(pltpu.VMEM((experts, LAST_ROWS, lanes), BF), pltpu.SemaphoreType.DMA((2,))),
-        far=(0,),
+        [((experts, GROUP, last_width), BF), ((5 * channels + experts, tokens), F32)],
+        (lifted, w_out, mix, saved, ends),
+        scratch=(
+            pltpu.VMEM((experts, GROUP, last_width), BF),
+            pltpu.VMEM((5 * channels + experts, tokens), F32),
+            pltpu.SemaphoreType.DMA((3,)),
+        ),
+        far=(0, 1),
     )
     piece, acts = lax.optimization_barrier((piece, acts))
     grads = expert_grads(whole, acts, width)
@@ -519,7 +553,8 @@
     g_proj, g_conv, g_branch = call(
         finish_body,
         [((width // experts, channels), F32), ((channels, tokens), F32), ((channels, tokens), F32)],
-        (last, ends, saved, kept),
+        (kept, last, saved),
+        fetched=1,
         scratch=(pltpu.VMEM((experts, tokens), F32),),
     )
     return (grads[0], grads[1], grads[2], g_proj, g_conv, g_branch)

time: 172 us -> 169 us (0.983)
  no operation moved by 1% of the time
where the time goes in v2:
time: 169 us
  blocking collectives  130 us (77%)
  waiting for transfers between devices  19.1 us (11%)
  Pallas kernels  13.5 us (8%)
  starting transfers between devices  6.07 us (4%)
    all_to_all x1, blocking collectives, local(): whole = lax.all_to_all(spread, 'tp', 0, 0, tiled=True)  39.1 us
    all_to_all x1, blocking collectives, local(): got = lax.all_to_all(sent, 'sp', split_axis=0, concat_axis=0, tiled=True)  33.7 us
    all_to_all x1, blocking collectives, local(): lax.all_to_all(returned.reshape(experts, HOME_ROWS, lanes), 'sp', split_a...  24.4 us
    all_to_all x1, blocking collectives, local(): parts = lax.all_to_all(dxp, 'tp', 0, 0, tiled=True)  19.8 us
    all_to_all x1, waiting for transfers between devices, local(): last = lax.all_to_all(piece, 'sp', split_axis=0, concat_axis=0, tiled=True)  19.1 us
    all_to_all x1, blocking collectives, local(): lifted = lax.all_to_all(own, 'tp', 0, 0, tiled=True)  12.6 us
    pallas_call x7, Pallas kernels, call(): pl.pallas_call(body, out_shape=[pltpu.HBM(*out) if k in far else jax.Shap...  9.36 us
    all_to_all x1, starting transfers between devices, local(): last = lax.all_to_all(piece, 'sp', split_axis=0, concat_axis=0, tiled=True)  6.07 us
  transfers between devices with their start and end apart: 1, of which 1 were waited for; matrix products, arithmetic and copies ran while one was open for 0% of the time, Pallas kernels for 2%

profile of v2, /device:TPU:1, one launch (start us, length us, event | category | flops | bytes accessed | tf_op | source)
XLA Modules:
  0.0 168.9 jit_solution(18266619710117152847)
XLA Ops:
  0.6 1.4 shard_map.172
  2.0 33.7 %all_to_all.30.refs_0_ = bf16[32,4,640]{2,1,0:T(4,128)(2,1)S(1)} all-to-all(bf16[32,4,640]{2,1,0:T(4,128)(2,1)S(1)} %get-tuple-element.25), channel_id=1, replica_groups=mesh['sp'=32,'tp'=16] {'sp'}, dimensions={0} | all-to-all | bytes 327680 | tf_op jit(solution)/shard_map/all_to_all | solution.py:487
  35.7 0.7 shard_map.173
  36.4 0.0 copy-start
  36.4 0.0 copy-start.1
  36.4 0.0 copy-start.2
  36.4 39.1 %all_to_all.31.refs_5_.whole = bf16[16,640,128]{2,1,0:T(8,128)(2,1)S(1)} all-to-all(bf16[16,640,128]{2,1,0:T(8,128)(2,1)S(1)} %shard_map.173), channel_id=1, replica_groups=mesh['sp'=32,'tp'=16] {'tp'}, dimensions={0} | all-to-all | bytes 5242880 | tf_op jit(solution)/shard_map/all_to_all | solution.py:493
  75.5 0.0 copy-done
  75.5 0.0 copy-done.1
  75.5 0.0 copy-done.2
  75.5 2.5 %shard_map.174 = (bf16[16,320,128]{2,1,0:T(8,128)(2,1)S(1)}, bf16[320,384]{1,0:T(8,128)(2,1)}, f32[12,64,128]{2,1,0:T(8,128)S(1)}, bf16[8,128]{1,0:T(8,128)(2,1)S(1)}) custom-call(bf16[64,128]{1,0:T(8,128)(2,1)} %refs_0_.1, bf16[64,128]{1,0:T(8,128)(2,1)} %refs_1_.1, bf16[1,64,64]{2,1,0:T(8,128)(2,1)} %refs_2_.3, bf16[1,64,64]{2,1,0:T(8,128)(2,1)} %refs_3_.3, ...), custom_call_target="tpu_custom_call" | custom-call | flops 838860800 | bytes 1 | tf_op jit(solution)/shard_map/pallas_call | solution.py:39
  78.0 0.0 copy-start.5
  78.0 0.0 copy-start.3
  78.0 19.8 %all_to_all.32.refs_0_ = bf16[16,320,128]{2,1,0:T(8,128)(2,1)S(1)} all-to-all(bf16[16,320,128]{2,1,0:T(8,128)(2,1)S(1)} %get-tuple-element.26), channel_id=1, replica_groups=mesh['sp'=32,'tp'=16] {'tp'}, dimensions={0} | all-to-all | bytes 2621440 | tf_op jit(solution)/shard_map/all_to_all | solution.py:518
  97.8 0.0 copy-start.4
  97.8 0.5 shard_map.175
  98.3 24.4 %all_to_all.33 = bf16[32,16,128]{2,1,0:T(8,128)(2,1)S(1)} all-to-all(bf16[32,16,128]{2,1,0:T(8,128)(2,1)S(1)} %bitcast.12), channel_id=1, replica_groups=mesh['sp'=32,'tp'=16] {'sp'}, dimensions={0} | all-to-all | bytes 262144 | tf_op jit(solution)/shard_map/all_to_all | solution.py:524
  122.6 0.0 copy-done.5
  122.6 0.5 shard_map.176
  123.1 12.6 %all_to_all.34.lifted = bf16[16,128,128]{2,1,0:T(8,128)(2,1)S(1)} all-to-all(bf16[16,128,128]{2,1,0:T(8,128)(2,1)S(1)} %get-tuple-element.30), channel_id=1, replica_groups=mesh['sp'=32,'tp'=16] {'tp'}, dimensions={0} | all-to-all | bytes 1048576 | tf_op jit(solution)/shard_map/all_to_all | solution.py:537
  135.7 0.0 copy-done.3
  135.7 1.8 %shard_map.177 = (bf16[32,4,1152]{2,1,0:T(4,128)(2,1)}, f32[352,128]{1,0:T(8,128)}) custom-call(bf16[16,128,128]{2,1,0:T(8,128)(2,1)S(1)} %all_to_all.34.lifted, bf16[64,2048]{1,0:T(8,128)(2,1)S(1)} %copy-done.3, bf16[64,128]{1,0:T(8,128)(2,1)S(1)} %get-tuple-element.31.mix, f32[12,64,128]{2,1,0:T(8,128)S(1)} %get-tuple-element.29.saved, ...), custom_call_target="tpu_custom_call" | custom-call | flops 1 | bytes 1 | tf_op jit(solution)/shard_map/pallas_call | solution.py:39
  137.6 6.1 %all-to-all-start.5 = ((bf16[32,4,1152]{2,1,0:T(4,128)(2,1)}), bf16[32,4,1152]{2,1,0:T(4,128)(2,1)S(1)}, u32[]{:S(2)}, u32[]{:S(2)}) async-start(bf16[32,4,1152]{2,1,0:T(4,128)(2,1)} %get-tuple-element.40), calls=%async_computation.5 | async-start | bytes 589824 | tf_op jit(solution)/shard_map/all_to_all | solution.py:552
  143.7 0.0 copy-done.4
  143.7 4.1 %shard_map.178 = (bf16[1,128,2048]{2,1,0:T(8,128)(2,1)}, bf16[1,128,2048]{2,1,0:T(8,128)(2,1)}, bf16[1,128,2048]{2,1,0:T(8,128)(2,1)}) custom-call(bf16[16,640,128]{2,1,0:T(8,128)(2,1)S(1)} %all_to_all.31.refs_5_.whole, bf16[320,384]{1,0:T(8,128)(2,1)S(1)} %copy-done.4), custom_call_target="tpu_custom_call" | custom-call | flops 503316480 | bytes 1572864 | tf_op jit(solution)/shard_map/pallas_call | solution.py:187
  147.8 19.1 %all-to-all-done.5.last = bf16[32,4,1152]{2,1,0:T(4,128)(2,1)S(1)} async-done(((bf16[32,4,1152]{2,1,0:T(4,128)(2,1)}), bf16[32,4,1152]{2,1,0:T(4,128)(2,1)S(1)}, u32[]{:S(2)}, u32[]{:S(2)}) %all-to-all-start.5) | async-done | bytes 294944 | tf_op jit(solution)/shard_map/all_to_all | solution.py:552
  166.9 2.0 %shard_map.179 = (f32[64,64]{1,0:T(8,128)}, f32[64,128]{1,0:T(8,128)}, f32[64,128]{1,0:T(8,128)}) custom-call(f32[352,128]{1,0:T(8,128)} %get-tuple-element.39.far_kept, bf16[32,4,1152]{2,1,0:T(4,128)(2,1)S(1)} %all-to-all-done.5.last, f32[12,64,128]{2,1,0:T(8,128)S(1)} %get-tuple-element.29.saved), custom_call_target="tpu_custom_call" | custom-call | flops 1 | bytes 1 | tf_op jit(solution)/shard_map/pallas_call | solution.py:39
Async XLA Ops:
  36.4 39.1 %copy-start = (bf16[1,128,2048]{2,1,0:T(8,128)(2,1)S(1)}, bf16[1,128,2048]{2,1,0:T(8,128)(2,1)}, u32[]{:S(2)}) copy-start(bf16[1,128,2048]{2,1,0:T(8,128)(2,1)} %param.17) | copy-start | bytes 1572868
  36.4 39.1 %copy-start.1 = (bf16[1,128,2048]{2,1,0:T(8,128)(2,1)S(1)}, bf16[1,128,2048]{2,1,0:T(8,128)(2,1)}, u32[]{:S(2)}) copy-start(bf16[1,128,2048]{2,1,0:T(8,128)(2,1)} %param.18) | copy-start | bytes 1572868
  36.4 39.1 %copy-start.2 = (bf16[1,128,2048]{2,1,0:T(8,128)(2,1)S(1)}, bf16[1,128,2048]{2,1,0:T(8,128)(2,1)}, u32[]{:S(2)}) copy-start(bf16[1,128,2048]{2,1,0:T(8,128)(2,1)} %param.19) | copy-start | bytes 1572868
  78.0 44.7 %copy-start.5 = (bf16[128,128]{1,0:T(8,128)(2,1)S(1)}, bf16[128,128]{1,0:T(8,128)(2,1)}, u32[]{:S(2)}) copy-start(bf16[128,128]{1,0:T(8,128)(2,1)} %cot.1) | copy-start | bytes 98308
  78.0 57.7 %copy-start.3 = (bf16[64,2048]{1,0:T(8,128)(2,1)S(1)}, bf16[64,2048]{1,0:T(8,128)(2,1)}, u32[]{:S(2)}) copy-start(bf16[64,2048]{1,0:T(8,128)(2,1)} %w_out.1) | copy-start | bytes 786436
  97.8 45.9 %copy-start.4 = (bf16[320,384]{1,0:T(8,128)(2,1)S(1)}, bf16[320,384]{1,0:T(8,128)(2,1)}, u32[]{:S(2)}) copy-start(bf16[320,384]{1,0:T(8,128)(2,1)} %get-tuple-element.35.acts) | copy-start | bytes 737284
  137.6 29.3 %all-to-all-start.5 = ((bf16[32,4,1152]{2,1,0:T(4,128)(2,1)}), bf16[32,4,1152]{2,1,0:T(4,128)(2,1)S(1)}, u32[]{:S(2)}, u32[]{:S(2)}) async-start(bf16[32,4,1152]{2,1,0:T(4,128)(2,1)} %get-tuple-element.40), calls=%async_computation.5 | async-start | bytes 589824 | tf_op jit(solution)/shard_map/all_to_all | solution.py:552

commit v3 on v2

--- a/solution.py
+++ b/solution.py
@@ -353,33 +353,36 @@
     mix[...] = (saved[5] * (fwd + bwd)).astype(BF)
 
 
-def in_groups(out, spot, rows):
-    width = rows.shape[1]
-    for k in range(rows.shape[0] // GROUP):
-        out[spot, :, width * k : width * (k + 1)] = rows[GROUP * k : GROUP * (k + 1)].astype(BF)
-
-
-def last_body(lifted, w_out, mix, saved, ends, far_out, far_kept, out, kept, sems):
+def proj_body(lifted, mix, mine, theirs):
     blocks, tokens, _ = lifted.shape
     channels = mix.shape[0]
     half = channels // 2
+    part_rows = mine.shape[1]
+    left = iota((half, 128), 1) < 64
+    even = (lax.axis_index("sp") & 1) == 0
+    mixed = mix[...]
+    for k in range(blocks // 2):
+        proj = dot(mixed, pair(lifted, k, 0, tokens))
+        for q in range(2):
+            part = proj[:, 128 * q : 128 * (q + 1)]
+            top, bottom = part[:half], part[half:]
+            spot = 4 * k + 2 * q
+            first = jnp.where(left, top, pltpu.roll(bottom, 64, 1))
+            second = jnp.where(left, pltpu.roll(top, 64, 1), bottom)
+            for n, rows in enumerate((first, second)):
+                low, high = rows[:part_rows], rows[part_rows:]
+                mine[spot + n] = jnp.where(even, low, high)
+                theirs[spot + n] = jnp.where(even, high, low).astype(BF)
+
+
+def adjoint_body(lifted, w_out, saved, ends, far_kept, carry, kept, sem):
+    blocks, tokens, _ = lifted.shape
+    channels = w_out.shape[0]
     lane = iota((channels, tokens), 1)
-    left = iota((half, 128), 1) < 64
-    mixed = mix[...]
     mix_cot = jnp.zeros((channels, tokens), F32)
     for k in range(blocks // 2):
         both = pair(lifted, k, 0, tokens)
         mix_cot = mix_cot + dot(w_out[:, 256 * k : 256 * (k + 1)], both, 1, 1)
-        proj = dot(mixed, both)
-        for q in range(2):
-            part = proj[:, 128 * q : 128 * (q + 1)]
-            top, bottom = part[:half], part[half:]
-            spot = 4 * k + 2 * q
-            in_groups(out, spot, jnp.where(left, top, pltpu.roll(bottom, 64, 1)))
-            in_groups(out, spot + 1, jnp.where(left, pltpu.roll(top, 64, 1), bottom))
-    cut = half // GROUP * 128
-    first = pltpu.make_async_copy(out.at[:, :, :cut], far_out.at[:, :, :cut], sems.at[0])
-    first.start()
     decay = saved[0]
     cot = mix_cot * saved[5]
     weighted = decay * cot
@@ -390,21 +393,29 @@
     kept[2 * channels : 3 * channels] = up
     kept[3 * channels : 4 * channels] = down
     kept[4 * channels :] = ends[...]
-    third = pltpu.make_async_copy(kept, far_kept, sems.at[2])
-    third.start()
+    write = pltpu.make_async_copy(kept, far_kept, sem)
+    write.start()
     rows = in_three(ends_row(up, down, lane))
     place = iota((8, tokens), 0)
     total = jnp.zeros((8, tokens), F32)
     for k, row in enumerate(rows):
         total = jnp.where(place == k, row.astype(F32), total)
-    total = total[:GROUP].astype(BF)
-    for s in range(out.shape[0]):
-        out[s, :, cut:] = total
-    second = pltpu.make_async_copy(out.at[:, :, cut:], far_out.at[:, :, cut:], sems.at[1])
-    second.start()
-    first.wait()
-    third.wait()
-    second.wait()
+    carry[...] = total
+    write.wait()
+
+
+def pack_body(mine, theirs, carry, far_out, out, sem):
+    devices, part_rows, width = mine.shape
+    tail = carry[...][:GROUP].astype(BF)
+    for s in range(devices):
+        rows = mine[s] + theirs[s].astype(F32)
+        for k in range(part_rows // GROUP):
+            group = rows[GROUP * k : GROUP * (k + 1)].astype(BF)
+            out[s, :, width * k : width * (k + 1)] = group
+        out[s, :, width * (part_rows // GROUP) :] = tail
+    write = pltpu.make_async_copy(out, far_out, sem)
+    write.start()
+    write.wait()
 
 
 def finish_body(far_kept, last, saved, g_proj, g_conv, g_branch, kept, adds, sems):
@@ -413,15 +424,15 @@
     channels, tokens = g_conv.shape
     ends = kept.at[4 * channels :, :]
     prods = kept.at[5 * channels :, :]
-    half = channels // 2
     lane = iota((channels, tokens), 1)
-    cut = half // GROUP * 128
-    total = last[0, :, :cut].astype(F32)
+    cut = last.shape[2] - 128
+    totals = [jnp.zeros((GROUP, cut), F32)] * 2
     for s in range(devices):
-        if s:
-            total = total + last[s, :, :cut].astype(F32)
+        totals[s & 1] = totals[s & 1] + last[s, :, :cut].astype(F32)
         adds[s : s + 1, :] = jnp.sum(last[s, :, cut:].astype(F32), axis=0, keepdims=True)
-    turned = jnp.concatenate([total[:, k : k + 128] for k in range(0, cut, 128)], axis=0).T
+    turned = jnp.concatenate(
+        [total[:, k : k + 128] for total in totals for k in range(0, cut, 128)], axis=0
+    ).T
     g_proj[...] = jnp.concatenate([turned[:64], turned[64:]], axis=1)
     copy.wait()
     adj_in, adj_back = to_columns(fold(lax.axis_index("sp"), prods, adds, channels), lane)
@@ -535,17 +546,29 @@
         scratch=(pltpu.VMEM((experts, tokens), F32),),
     )
     lifted = lax.all_to_all(own, "tp", 0, 0, tiled=True)
-    last_width = (channels // 2 // GROUP + 1) * lanes
-    piece, kept = call(
-        last_body,
-        [((experts, GROUP, last_width), BF), ((5 * channels + experts, tokens), F32)],
-        (lifted, w_out, mix, saved, ends),
-        scratch=(
-            pltpu.VMEM((experts, GROUP, last_width), BF),
-            pltpu.VMEM((5 * channels + experts, tokens), F32),
-            pltpu.SemaphoreType.DMA((3,)),
-        ),
-        far=(0, 1),
+    part_rows = channels // 4
+    last_width = (part_rows // GROUP + 1) * lanes
+    mine, theirs = call(
+        proj_body,
+        [((experts, part_rows, lanes), F32), ((experts, part_rows, lanes), BF)],
+        (lifted, mix),
+        flops=2 * channels * tokens * width,
+    )
+    swapped = lax.ppermute(theirs, "sp", [(i, i ^ 1) for i in range(experts)])
+    kept, last_carry = call(
+        adjoint_body,
+        [((5 * channels + experts, tokens), F32), ((8, tokens), F32)],
+        (lifted, w_out, saved, ends),
+        flops=100 * channels * tokens * width,
+        scratch=(pltpu.VMEM((5 * channels + experts, tokens), F32), pltpu.SemaphoreType.DMA),
+        far=(0,),
+    )
+    (piece,) = call(
+        pack_body,
+        [((experts, GROUP, last_width), BF)],
+        (mine, swapped, last_carry),
+        scratch=(pltpu.VMEM((experts, GROUP, last_width), BF), pltpu.SemaphoreType.DMA),
+        far=(0,),
     )
     piece, acts = lax.optimization_barrier((piece, acts))
     grads = expert_grads(whole, acts, width)

time: 169 us -> 166 us (0.982)
  waiting for transfers between devices: 19.1 us -> 13 us
  starting transfers between devices: 6.07 us -> 8.11 us
    all_to_all x1, waiting for transfers between devices: 19.1 us -> 13 us  [local(): last = lax.all_to_all(piece, 'sp', split_axis=0, concat_axis=0, tiled=True)]
    ppermute x0 -> x1, starting transfers between devices: none -> 4.45 us  [local(): swapped = lax.ppermute(theirs, 'sp', [(i, i ^ 1) for i in range(experts)])]
    all_to_all x1, starting transfers between devices: 6.07 us -> 3.66 us  [local(): last = lax.all_to_all(piece, 'sp', split_axis=0, concat_axis=0, tiled=True)]
    pallas_call x7 -> x9, Pallas kernels: 9.36 us -> 10.3 us  [call(): pl.pallas_call(body, out_shape=[pltpu.HBM(*out) if k in far else jax.Shap...]
  transfers between devices with their start and end apart: 1 -> 2, of which waited for: 1 -> 1; matrix products, arithmetic and copies ran while one was open for 0% -> 0% of each run, Pallas kernels for 2% -> 4%
where the time goes in v3:
time: 166 us
  blocking collectives  129 us (78%)
  Pallas kernels  14.4 us (9%)
  waiting for transfers between devices  13 us (8%)
  starting transfers between devices  8.11 us (5%)
    all_to_all x1, blocking collectives, local(): whole = lax.all_to_all(spread, 'tp', 0, 0, tiled=True)  39.1 us
    all_to_all x1, blocking collectives, local(): got = lax.all_to_all(sent, 'sp', split_axis=0, concat_axis=0, tiled=True)  33.7 us
    all_to_all x1, blocking collectives, local(): lax.all_to_all(returned.reshape(experts, HOME_ROWS, lanes), 'sp', split_a...  24.4 us
    all_to_all x1, blocking collectives, local(): parts = lax.all_to_all(dxp, 'tp', 0, 0, tiled=True)  19.7 us
    all_to_all x1, waiting for transfers between devices, local(): last = lax.all_to_all(piece, 'sp', split_axis=0, concat_axis=0, tiled=True)  13 us
    all_to_all x1, blocking collectives, local(): lifted = lax.all_to_all(own, 'tp', 0, 0, tiled=True)  12.6 us
    pallas_call x9, Pallas kernels, call(): pl.pallas_call(body, out_shape=[pltpu.HBM(*out) if k in far else jax.Shap...  10.3 us
    ppermute x1, starting transfers between devices, local(): swapped = lax.ppermute(theirs, 'sp', [(i, i ^ 1) for i in range(experts)])  4.45 us
  transfers between devices with their start and end apart: 2, of which 1 were waited for; matrix products, arithmetic and copies ran while one was open for 0% of the time, Pallas kernels for 4%

profile of v3, /device:TPU:1, one launch (start us, length us, event | category | flops | bytes accessed | tf_op | source)
XLA Modules:
  0.0 165.7 jit_solution(2730441108728326515)
XLA Ops:
  0.6 1.4 shard_map.172
  2.0 33.7 %all_to_all.30.refs_0_ = bf16[32,4,640]{2,1,0:T(4,128)(2,1)S(1)} all-to-all(bf16[32,4,640]{2,1,0:T(4,128)(2,1)S(1)} %get-tuple-element.27), channel_id=1, replica_groups=mesh['sp'=32,'tp'=16] {'sp'}, dimensions={0} | all-to-all | bytes 327680 | tf_op jit(solution)/shard_map/all_to_all | solution.py:498
  35.7 0.7 shard_map.173
  36.4 0.0 copy-start
  36.4 0.0 copy-start.1
  36.4 0.0 copy-start.2
  36.4 39.1 %all_to_all.31.refs_5_.whole = bf16[16,640,128]{2,1,0:T(8,128)(2,1)S(1)} all-to-all(bf16[16,640,128]{2,1,0:T(8,128)(2,1)S(1)} %shard_map.173), channel_id=1, replica_groups=mesh['sp'=32,'tp'=16] {'tp'}, dimensions={0} | all-to-all | bytes 5242880 | tf_op jit(solution)/shard_map/all_to_all | solution.py:504
  75.5 0.0 copy-done
  75.5 0.0 copy-done.1
  75.5 0.0 copy-done.2
  75.5 2.5 %shard_map.174 = (bf16[16,320,128]{2,1,0:T(8,128)(2,1)S(1)}, bf16[320,384]{1,0:T(8,128)(2,1)}, f32[12,64,128]{2,1,0:T(8,128)S(1)}, bf16[8,128]{1,0:T(8,128)(2,1)S(1)}) custom-call(bf16[64,128]{1,0:T(8,128)(2,1)} %refs_0_.1, bf16[64,128]{1,0:T(8,128)(2,1)} %refs_1_.1, bf16[1,64,64]{2,1,0:T(8,128)(2,1)} %refs_2_.3, bf16[1,64,64]{2,1,0:T(8,128)(2,1)} %refs_3_.3, ...), custom_call_target="tpu_custom_call" | custom-call | flops 838860800 | bytes 1 | tf_op jit(solution)/shard_map/pallas_call | solution.py:39
  78.0 0.0 copy-start.4
  78.0 19.7 %all_to_all.32.refs_0_ = bf16[16,320,128]{2,1,0:T(8,128)(2,1)S(1)} all-to-all(bf16[16,320,128]{2,1,0:T(8,128)(2,1)S(1)} %get-tuple-element.28), channel_id=1, replica_groups=mesh['sp'=32,'tp'=16] {'tp'}, dimensions={0} | all-to-all | bytes 2621440 | tf_op jit(solution)/shard_map/all_to_all | solution.py:529
  97.7 0.0 copy-start.5
  97.7 0.5 shard_map.175
  98.1 24.4 %all_to_all.33 = bf16[32,16,128]{2,1,0:T(8,128)(2,1)S(1)} all-to-all(bf16[32,16,128]{2,1,0:T(8,128)(2,1)S(1)} %bitcast.12), channel_id=1, replica_groups=mesh['sp'=32,'tp'=16] {'sp'}, dimensions={0} | all-to-all | bytes 262144 | tf_op jit(solution)/shard_map/all_to_all | solution.py:535
  122.5 0.0 copy-done.4
  122.5 0.5 shard_map.176
  123.0 12.6 %all_to_all.34.lifted = bf16[16,128,128]{2,1,0:T(8,128)(2,1)S(1)} all-to-all(bf16[16,128,128]{2,1,0:T(8,128)(2,1)S(1)} %get-tuple-element.32), channel_id=1, replica_groups=mesh['sp'=32,'tp'=16] {'tp'}, dimensions={0} | all-to-all | bytes 1048576 | tf_op jit(solution)/shard_map/all_to_all | solution.py:548
  135.6 0.4 shard_map.177
  135.9 4.5 %collective-permute-start = (bf16[32,16,128]{2,1,0:T(8,128)(2,1)S(1)}, bf16[32,16,128]{2,1,0:T(8,128)(2,1)S(1)}, u32[]{:S(2)}, u32[]{:S(2)}) collective-permute-start(bf16[32,16,128]{2,1,0:T(8,128)(2,1)S(1)} %get-tuple-element.35), channel_id=1, source_target_pairs={{0,16},{16,0},{32,48},{48,32},{64,80},{80,64},{96,112},{112,96},{1... | collective-permute-start | bytes 393224 | tf_op jit(solution)/shard_map/ppermute | solution.py:557
  140.4 0.0 copy-done.5
  140.4 0.0 copy-start.3
  140.4 1.7 %shard_map.178 = (f32[352,128]{1,0:T(8,128)}, f32[8,128]{1,0:T(8,128)S(1)}) custom-call(bf16[16,128,128]{2,1,0:T(8,128)(2,1)S(1)} %all_to_all.34.lifted, bf16[64,2048]{1,0:T(8,128)(2,1)S(1)} %copy-done.5, f32[12,64,128]{2,1,0:T(8,128)S(1)} %get-tuple-element.31.saved, f32[96,128]{1,0:T(8,128)S(1)} %get-tuple-element.36.ends), custom_call_target="tpu_custom_call" | custom-call | flops 1677721600 | bytes 1 | tf_op jit(solution)/shard_map/pallas_call | solution.py:39
  142.2 0.0 collective-permute-done.theirs
  142.2 0.7 shard_map.179
  142.9 3.7 %all-to-all-start.5 = ((bf16[32,4,640]{2,1,0:T(4,128)(2,1)}), bf16[32,4,640]{2,1,0:T(4,128)(2,1)S(1)}, u32[]{:S(2)}, u32[]{:S(2)}) async-start(bf16[32,4,640]{2,1,0:T(4,128)(2,1)} %shard_map.179), calls=%async_computation.5 | async-start | bytes 327680 | tf_op jit(solution)/shard_map/all_to_all | solution.py:575
  146.6 0.0 copy-done.3
  146.6 4.1 %shard_map.180 = (bf16[1,128,2048]{2,1,0:T(8,128)(2,1)}, bf16[1,128,2048]{2,1,0:T(8,128)(2,1)}, bf16[1,128,2048]{2,1,0:T(8,128)(2,1)}) custom-call(bf16[16,640,128]{2,1,0:T(8,128)(2,1)S(1)} %all_to_all.31.refs_5_.whole, bf16[320,384]{1,0:T(8,128)(2,1)S(1)} %copy-done.3), custom_call_target="tpu_custom_call" | custom-call | flops 503316480 | bytes 1572864 | tf_op jit(solution)/shard_map/pallas_call | solution.py:187
  150.7 13.0 %all-to-all-done.5.last = bf16[32,4,640]{2,1,0:T(4,128)(2,1)S(1)} async-done(((bf16[32,4,640]{2,1,0:T(4,128)(2,1)}), bf16[32,4,640]{2,1,0:T(4,128)(2,1)S(1)}, u32[]{:S(2)}, u32[]{:S(2)}) %all-to-all-start.5) | async-done | bytes 163872 | tf_op jit(solution)/shard_map/all_to_all | solution.py:575
  163.7 2.0 %shard_map.181 = (f32[64,64]{1,0:T(8,128)}, f32[64,128]{1,0:T(8,128)}, f32[64,128]{1,0:T(8,128)}) custom-call(f32[352,128]{1,0:T(8,128)} %get-tuple-element.43.far_kept, bf16[32,4,640]{2,1,0:T(4,128)(2,1)S(1)} %all-to-all-done.5.last, f32[12,64,128]{2,1,0:T(8,128)S(1)} %get-tuple-element.31.saved), custom_call_target="tpu_custom_call" | custom-call | flops 1 | bytes 1 | tf_op jit(solution)/shard_map/pallas_call | solution.py:39
Async XLA Ops:
  36.4 39.1 %copy-start = (bf16[1,128,2048]{2,1,0:T(8,128)(2,1)S(1)}, bf16[1,128,2048]{2,1,0:T(8,128)(2,1)}, u32[]{:S(2)}) copy-start(bf16[1,128,2048]{2,1,0:T(8,128)(2,1)} %param.17) | copy-start | bytes 1572868
  36.4 39.1 %copy-start.1 = (bf16[1,128,2048]{2,1,0:T(8,128)(2,1)S(1)}, bf16[1,128,2048]{2,1,0:T(8,128)(2,1)}, u32[]{:S(2)}) copy-start(bf16[1,128,2048]{2,1,0:T(8,128)(2,1)} %param.18) | copy-start | bytes 1572868
  36.4 39.1 %copy-start.2 = (bf16[1,128,2048]{2,1,0:T(8,128)(2,1)S(1)}, bf16[1,128,2048]{2,1,0:T(8,128)(2,1)}, u32[]{:S(2)}) copy-start(bf16[1,128,2048]{2,1,0:T(8,128)(2,1)} %param.19) | copy-start | bytes 1572868
  78.0 44.5 %copy-start.4 = (bf16[128,128]{1,0:T(8,128)(2,1)S(1)}, bf16[128,128]{1,0:T(8,128)(2,1)}, u32[]{:S(2)}) copy-start(bf16[128,128]{1,0:T(8,128)(2,1)} %cot.1) | copy-start | bytes 98308
  97.7 42.7 %copy-start.5 = (bf16[64,2048]{1,0:T(8,128)(2,1)S(1)}, bf16[64,2048]{1,0:T(8,128)(2,1)}, u32[]{:S(2)}) copy-start(bf16[64,2048]{1,0:T(8,128)(2,1)} %w_out.1) | copy-start | bytes 786436
  135.9 6.2 %collective-permute-start = (bf16[32,16,128]{2,1,0:T(8,128)(2,1)S(1)}, bf16[32,16,128]{2,1,0:T(8,128)(2,1)S(1)}, u32[]{:S(2)}, u32[]{:S(2)}) collective-permute-start(bf16[32,16,128]{2,1,0:T(8,128)(2,1)S(1)} %get-tuple-element.35), channel_id=1, source_target_pairs={{0,16},{16,0},{32,48},{48,32},{64,80},{80,64},{96,112},{112,96},{1... | collective-permute-start | bytes 393224 | tf_op jit(solution)/shard_map/ppermute | solution.py:557
  140.4 6.2 %copy-start.3 = (bf16[320,384]{1,0:T(8,128)(2,1)S(1)}, bf16[320,384]{1,0:T(8,128)(2,1)}, u32[]{:S(2)}) copy-start(bf16[320,384]{1,0:T(8,128)(2,1)} %get-tuple-element.39.acts) | copy-start | bytes 737284
  142.9 20.8 %all-to-all-start.5 = ((bf16[32,4,640]{2,1,0:T(4,128)(2,1)}), bf16[32,4,640]{2,1,0:T(4,128)(2,1)S(1)}, u32[]{:S(2)}, u32[]{:S(2)}) async-start(bf16[32,4,640]{2,1,0:T(4,128)(2,1)} %shard_map.179), calls=%async_computation.5 | async-start | bytes 327680 | tf_op jit(solution)/shard_map/all_to_all | solution.py:575

commit v4 on v3

--- a/solution.py
+++ b/solution.py
@@ -279,6 +279,7 @@
 
 
 SAVED = 12
+KEPT = 6
 
 
 def soft_plus(x):
@@ -375,7 +376,7 @@
                 theirs[spot + n] = jnp.where(even, high, low).astype(BF)
 
 
-def adjoint_body(lifted, w_out, saved, ends, far_kept, carry, kept, sem):
+def adjoint_body(lifted, w_out, saved, ends, kept):
     blocks, tokens, _ = lifted.shape
     channels = w_out.shape[0]
     lane = iota((channels, tokens), 1)
@@ -392,21 +393,19 @@
     kept[channels : 2 * channels] = cot
     kept[2 * channels : 3 * channels] = up
     kept[3 * channels : 4 * channels] = down
-    kept[4 * channels :] = ends[...]
-    write = pltpu.make_async_copy(kept, far_kept, sem)
-    write.start()
+    kept[4 * channels : 4 * channels + ends.shape[0]] = ends[...]
     rows = in_three(ends_row(up, down, lane))
     place = iota((8, tokens), 0)
     total = jnp.zeros((8, tokens), F32)
     for k, row in enumerate(rows):
         total = jnp.where(place == k, row.astype(F32), total)
-    carry[...] = total
-    write.wait()
-
-
-def pack_body(mine, theirs, carry, far_out, out, sem):
+    kept[kept.shape[0] - 8 :] = total
+
+
+def pack_body(mine, theirs, kept, far_out, out, sem):
     devices, part_rows, width = mine.shape
-    tail = carry[...][:GROUP].astype(BF)
+    spot = kept.shape[0] - 8
+    tail = kept[spot : spot + 8][:GROUP].astype(BF)
     for s in range(devices):
         rows = mine[s] + theirs[s].astype(F32)
         for k in range(part_rows // GROUP):
@@ -418,12 +417,11 @@
     write.wait()
 
 
-def finish_body(far_kept, last, saved, g_proj, g_conv, g_branch, kept, adds, sems):
-    (copy,) = fetch((far_kept,), (kept,), sems)
+def finish_body(last, saved, kept, g_proj, g_conv, g_branch, adds):
     devices = adds.shape[0]
     channels, tokens = g_conv.shape
     ends = kept.at[4 * channels :, :]
-    prods = kept.at[5 * channels :, :]
+    prods = kept.at[5 * channels : 5 * channels + devices, :]
     lane = iota((channels, tokens), 1)
     cut = last.shape[2] - 128
     totals = [jnp.zeros((GROUP, cut), F32)] * 2
@@ -434,7 +432,6 @@
         [total[:, k : k + 128] for total in totals for k in range(0, cut, 128)], axis=0
     ).T
     g_proj[...] = jnp.concatenate([turned[:64], turned[64:]], axis=1)
-    copy.wait()
     adj_in, adj_back = to_columns(fold(lax.axis_index("sp"), prods, adds, channels), lane)
     state_in, state_back = ends[:channels, :1], ends[:channels, tokens - 1 :]
     fwd, bwd = joined_states(saved, state_in, state_back)
@@ -555,18 +552,16 @@
         flops=2 * channels * tokens * width,
     )
     swapped = lax.ppermute(theirs, "sp", [(i, i ^ 1) for i in range(experts)])
-    kept, last_carry = call(
+    (kept,) = call(
         adjoint_body,
-        [((5 * channels + experts, tokens), F32), ((8, tokens), F32)],
+        [((KEPT * channels, tokens), F32)],
         (lifted, w_out, saved, ends),
         flops=100 * channels * tokens * width,
-        scratch=(pltpu.VMEM((5 * channels + experts, tokens), F32), pltpu.SemaphoreType.DMA),
-        far=(0,),
     )
     (piece,) = call(
         pack_body,
         [((experts, GROUP, last_width), BF)],
-        (mine, swapped, last_carry),
+        (mine, swapped, kept),
         scratch=(pltpu.VMEM((experts, GROUP, last_width), BF), pltpu.SemaphoreType.DMA),
         far=(0,),
     )
@@ -576,8 +571,7 @@
     g_proj, g_conv, g_branch = call(
         finish_body,
         [((width // experts, channels), F32), ((channels, tokens), F32), ((channels, tokens), F32)],
-        (kept, last, saved),
-        fetched=1,
+        (last, saved, kept),
         scratch=(pltpu.VMEM((experts, tokens), F32),),
     )
     return (grads[0], grads[1], grads[2], g_proj, g_conv, g_branch)

time: 166 us -> 165 us (level)
  transfers between devices with their start and end apart: 2 -> 2, of which waited for: 1 -> 1; matrix products, arithmetic and copies ran while one was open for 0% -> 0% of each run, Pallas kernels for 4% -> 3%
where the time goes in v4:
time: 165 us; the launch traced here: 164 us
  blocking collectives  129 us (78%)
  Pallas kernels  13 us (8%)
  waiting for transfers between devices  12.2 us (7%)
  starting transfers between devices  8.12 us (5%)
    all_to_all x1, blocking collectives, local(): whole = lax.all_to_all(spread, 'tp', 0, 0, tiled=True)  39.1 us
    all_to_all x1, blocking collectives, local(): got = lax.all_to_all(sent, 'sp', split_axis=0, concat_axis=0, tiled=True)  33.7 us
    all_to_all x1, blocking collectives, local(): lax.all_to_all(returned.reshape(experts, HOME_ROWS, lanes), 'sp', split_a...  24.4 us
    all_to_all x1, blocking collectives, local(): parts = lax.all_to_all(dxp, 'tp', 0, 0, tiled=True)  19.7 us
    all_to_all x1, blocking collectives, local(): lifted = lax.all_to_all(own, 'tp', 0, 0, tiled=True)  12.6 us
    all_to_all x1, waiting for transfers between devices, local(): last = lax.all_to_all(piece, 'sp', split_axis=0, concat_axis=0, tiled=True)  12.2 us
    pallas_call x9, Pallas kernels, call(): pl.pallas_call(body, out_shape=[pltpu.HBM(*out) if k in far else jax.Shap...  8.85 us
    ppermute x1, starting transfers between devices, local(): swapped = lax.ppermute(theirs, 'sp', [(i, i ^ 1) for i in range(experts)])  4.45 us
  transfers between devices with their start and end apart: 2, of which 1 were waited for; matrix products, arithmetic and copies ran while one was open for 0% of the time, Pallas kernels for 3%

profile of v4, /device:TPU:1, one launch (start us, length us, event | category | flops | bytes accessed | tf_op | source)
XLA Modules:
  0.0 164.3 jit_solution(2515541741968058669)
XLA Ops:
  0.6 1.4 shard_map.172
  2.0 33.7 %all_to_all.30.refs_0_ = bf16[32,4,640]{2,1,0:T(4,128)(2,1)S(1)} all-to-all(bf16[32,4,640]{2,1,0:T(4,128)(2,1)S(1)} %get-tuple-element.25), channel_id=1, replica_groups=mesh['sp'=32,'tp'=16] {'sp'}, dimensions={0} | all-to-all | bytes 327680 | tf_op jit(solution)/shard_map/all_to_all | solution.py:495
  35.7 0.7 shard_map.173
  36.4 0.0 copy-start
  36.4 0.0 copy-start.1
  36.4 0.0 copy-start.2
  36.4 39.1 %all_to_all.31.refs_5_.whole = bf16[16,640,128]{2,1,0:T(8,128)(2,1)S(1)} all-to-all(bf16[16,640,128]{2,1,0:T(8,128)(2,1)S(1)} %shard_map.173), channel_id=1, replica_groups=mesh['sp'=32,'tp'=16] {'tp'}, dimensions={0} | all-to-all | bytes 5242880 | tf_op jit(solution)/shard_map/all_to_all | solution.py:501
  75.5 0.0 copy-done
  75.5 0.0 copy-done.1
  75.5 0.0 copy-done.2
  75.5 2.5 %shard_map.174 = (bf16[16,320,128]{2,1,0:T(8,128)(2,1)S(1)}, bf16[320,384]{1,0:T(8,128)(2,1)}, f32[12,64,128]{2,1,0:T(8,128)S(1)}, bf16[8,128]{1,0:T(8,128)(2,1)S(1)}) custom-call(bf16[64,128]{1,0:T(8,128)(2,1)} %refs_0_.1, bf16[64,128]{1,0:T(8,128)(2,1)} %refs_1_.1, bf16[1,64,64]{2,1,0:T(8,128)(2,1)} %refs_2_.3, bf16[1,64,64]{2,1,0:T(8,128)(2,1)} %refs_3_.3, ...), custom_call_target="tpu_custom_call" | custom-call | flops 838860800 | bytes 1 | tf_op jit(solution)/shard_map/pallas_call | solution.py:39
  78.0 0.0 copy-start.4
  78.0 19.7 %all_to_all.32.refs_0_ = bf16[16,320,128]{2,1,0:T(8,128)(2,1)S(1)} all-to-all(bf16[16,320,128]{2,1,0:T(8,128)(2,1)S(1)} %get-tuple-element.26), channel_id=1, replica_groups=mesh['sp'=32,'tp'=16] {'tp'}, dimensions={0} | all-to-all | bytes 2621440 | tf_op jit(solution)/shard_map/all_to_all | solution.py:526
  97.7 0.0 copy-start.5
  97.7 0.5 shard_map.175
  98.1 24.4 %all_to_all.33 = bf16[32,16,128]{2,1,0:T(8,128)(2,1)S(1)} all-to-all(bf16[32,16,128]{2,1,0:T(8,128)(2,1)S(1)} %bitcast.12), channel_id=1, replica_groups=mesh['sp'=32,'tp'=16] {'sp'}, dimensions={0} | all-to-all | bytes 262144 | tf_op jit(solution)/shard_map/all_to_all | solution.py:532
  122.5 0.0 copy-done.4
  122.5 0.5 shard_map.176
  123.0 12.6 %all_to_all.34.lifted = bf16[16,128,128]{2,1,0:T(8,128)(2,1)S(1)} all-to-all(bf16[16,128,128]{2,1,0:T(8,128)(2,1)S(1)} %get-tuple-element.30), channel_id=1, replica_groups=mesh['sp'=32,'tp'=16] {'tp'}, dimensions={0} | all-to-all | bytes 1048576 | tf_op jit(solution)/shard_map/all_to_all | solution.py:545
  135.6 0.4 shard_map.177
  135.9 4.5 %collective-permute-start = (bf16[32,16,128]{2,1,0:T(8,128)(2,1)S(1)}, bf16[32,16,128]{2,1,0:T(8,128)(2,1)S(1)}, u32[]{:S(2)}, u32[]{:S(2)}) collective-permute-start(bf16[32,16,128]{2,1,0:T(8,128)(2,1)S(1)} %get-tuple-element.33), channel_id=1, source_target_pairs={{0,16},{16,0},{32,48},{48,32},{64,80},{80,64},{96,112},{112,96},{1... | collective-permute-start | bytes 393224 | tf_op jit(solution)/shard_map/ppermute | solution.py:554
  140.4 0.0 copy-done.5
  140.4 1.1 shard_map.178.kept
  141.6 0.0 collective-permute-done.theirs
  141.6 0.8 shard_map.179
  142.3 3.7 %all-to-all-start.5 = ((bf16[32,4,640]{2,1,0:T(4,128)(2,1)}), bf16[32,4,640]{2,1,0:T(4,128)(2,1)S(1)}, u32[]{:S(2)}, u32[]{:S(2)}) async-start(bf16[32,4,640]{2,1,0:T(4,128)(2,1)} %shard_map.179), calls=%async_computation.5 | async-start | bytes 327680 | tf_op jit(solution)/shard_map/all_to_all | solution.py:570
  146.0 0.0 copy-start.3
  146.0 0.9 copy-done.3
  146.9 4.1 %shard_map.180 = (bf16[1,128,2048]{2,1,0:T(8,128)(2,1)}, bf16[1,128,2048]{2,1,0:T(8,128)(2,1)}, bf16[1,128,2048]{2,1,0:T(8,128)(2,1)}) custom-call(bf16[16,640,128]{2,1,0:T(8,128)(2,1)S(1)} %all_to_all.31.refs_5_.whole, bf16[320,384]{1,0:T(8,128)(2,1)S(1)} %copy-done.3), custom_call_target="tpu_custom_call" | custom-call | flops 503316480 | bytes 1572864 | tf_op jit(solution)/shard_map/pallas_call | solution.py:187
  151.0 12.2 %all-to-all-done.5.last = bf16[32,4,640]{2,1,0:T(4,128)(2,1)S(1)} async-done(((bf16[32,4,640]{2,1,0:T(4,128)(2,1)}), bf16[32,4,640]{2,1,0:T(4,128)(2,1)S(1)}, u32[]{:S(2)}, u32[]{:S(2)}) %all-to-all-start.5) | async-done | bytes 163872 | tf_op jit(solution)/shard_map/all_to_all | solution.py:570
  163.2 1.1 shard_map.181
Async XLA Ops:
  36.4 39.1 %copy-start = (bf16[1,128,2048]{2,1,0:T(8,128)(2,1)S(1)}, bf16[1,128,2048]{2,1,0:T(8,128)(2,1)}, u32[]{:S(2)}) copy-start(bf16[1,128,2048]{2,1,0:T(8,128)(2,1)} %param.17) | copy-start | bytes 1572868
  36.4 39.1 %copy-start.1 = (bf16[1,128,2048]{2,1,0:T(8,128)(2,1)S(1)}, bf16[1,128,2048]{2,1,0:T(8,128)(2,1)}, u32[]{:S(2)}) copy-start(bf16[1,128,2048]{2,1,0:T(8,128)(2,1)} %param.18) | copy-start | bytes 1572868
  36.4 39.1 %copy-start.2 = (bf16[1,128,2048]{2,1,0:T(8,128)(2,1)S(1)}, bf16[1,128,2048]{2,1,0:T(8,128)(2,1)}, u32[]{:S(2)}) copy-start(bf16[1,128,2048]{2,1,0:T(8,128)(2,1)} %param.19) | copy-start | bytes 1572868
  78.0 44.5 %copy-start.4 = (bf16[128,128]{1,0:T(8,128)(2,1)S(1)}, bf16[128,128]{1,0:T(8,128)(2,1)}, u32[]{:S(2)}) copy-start(bf16[128,128]{1,0:T(8,128)(2,1)} %cot.1) | copy-start | bytes 98308
  97.7 42.7 %copy-start.5 = (bf16[64,2048]{1,0:T(8,128)(2,1)S(1)}, bf16[64,2048]{1,0:T(8,128)(2,1)}, u32[]{:S(2)}) copy-start(bf16[64,2048]{1,0:T(8,128)(2,1)} %w_out.1) | copy-start | bytes 786436
  135.9 5.6 %collective-permute-start = (bf16[32,16,128]{2,1,0:T(8,128)(2,1)S(1)}, bf16[32,16,128]{2,1,0:T(8,128)(2,1)S(1)}, u32[]{:S(2)}, u32[]{:S(2)}) collective-permute-start(bf16[32,16,128]{2,1,0:T(8,128)(2,1)S(1)} %get-tuple-element.33), channel_id=1, source_target_pairs={{0,16},{16,0},{32,48},{48,32},{64,80},{80,64},{96,112},{112,96},{1... | collective-permute-start | bytes 393224 | tf_op jit(solution)/shard_map/ppermute | solution.py:554
  142.3 20.9 %all-to-all-start.5 = ((bf16[32,4,640]{2,1,0:T(4,128)(2,1)}), bf16[32,4,640]{2,1,0:T(4,128)(2,1)S(1)}, u32[]{:S(2)}, u32[]{:S(2)}) async-start(bf16[32,4,640]{2,1,0:T(4,128)(2,1)} %shard_map.179), calls=%async_computation.5 | async-start | bytes 327680 | tf_op jit(solution)/shard_map/all_to_all | solution.py:570
  146.0 0.9 copy-start.3

commit v5 on v4

--- a/solution.py
+++ b/solution.py
@@ -248,12 +248,21 @@
     return high, mid, low
 
 
-def ends_row(up, down, lane):
+def ends_rows(up, down, lane):
     width = up.shape[1]
     ends = jnp.concatenate(
         [jnp.where(lane == width - 1, up, 0.0), jnp.where(lane == 0, down, 0.0)], axis=0
     )
-    return dot(jnp.ones((8, width), F32), ends, 1, 1, lax.Precision.HIGHEST)
+    ones = jnp.ones((8, width), BF)
+    return [dot(ones, piece, 1, 1) for piece in in_three(ends)]
+
+
+def stacked(rows, width):
+    place = iota((8, width), 0)
+    total = jnp.zeros((8, width), F32)
+    for k, row in enumerate(rows):
+        total = jnp.where(place == k, row, total)
+    return total
 
 
 def to_columns(row, lane):
@@ -266,16 +275,19 @@
 
 def fold(me, prods, adds, channels):
     devices, width = prods.shape
-    lane = iota((1, width), 1)
+    row, lane = iota((devices, width), 0), iota((devices, width), 1)
     ahead = lane < channels
-    total = jnp.zeros((1, width), F32)
-    for n in range(devices):
-        m = devices - 1 - n
-        prod = jnp.where(ahead, prods[n : n + 1, :], prods[m : m + 1, :])
-        add = jnp.where(ahead, adds[n : n + 1, :], adds[m : m + 1, :])
-        live = jnp.where(ahead, (me > n).astype(I32), (me < m).astype(I32)) > 0
-        total = jnp.where(live, prod * total + add, total)
-    return total
+    live = jnp.where(ahead, (row < me).astype(I32), (row > me).astype(I32)) > 0
+    prod = jnp.where(live, prods[...], 1.0)
+    add = jnp.where(live, adds[...], 0.0)
+    d = 1
+    while d < devices:
+        next_prod = pltpu.roll(prod, devices - d, 0)
+        next_add = pltpu.roll(add, devices - d, 0)
+        add = jnp.where(ahead, next_prod * add + next_add, prod * next_add + add)
+        prod = prod * next_prod
+        d *= 2
+    return add[:1]
 
 
 SAVED = 12
@@ -322,14 +334,8 @@
     saved[9] = root * values * sig_a * (1.0 - sig_a)
     saved[10] = direct
     saved[11] = jnp.concatenate([w_recur[0], w_input[0]], axis=1).astype(F32)
-    rows = in_three(ends_row(up_prod, down_prod, lane)) + in_three(
-        ends_row(up_state, down_state, lane)
-    )
-    place = iota((8, tokens), 0)
-    total = jnp.zeros((8, tokens), F32)
-    for k, row in enumerate(rows):
-        total = jnp.where(place == k, row.astype(F32), total)
-    carry[...] = total.astype(BF)
+    rows = ends_rows(up_prod, down_prod, lane) + ends_rows(up_state, down_state, lane)
+    carry[...] = stacked(rows, tokens).astype(BF)
 
 
 def joined_states(saved, state_in, state_back):
@@ -394,27 +400,27 @@
     kept[2 * channels : 3 * channels] = up
     kept[3 * channels : 4 * channels] = down
     kept[4 * channels : 4 * channels + ends.shape[0]] = ends[...]
-    rows = in_three(ends_row(up, down, lane))
-    place = iota((8, tokens), 0)
-    total = jnp.zeros((8, tokens), F32)
-    for k, row in enumerate(rows):
-        total = jnp.where(place == k, row.astype(F32), total)
-    kept[kept.shape[0] - 8 :] = total
-
-
-def pack_body(mine, theirs, kept, far_out, out, sem):
+    kept[kept.shape[0] - 8 :] = stacked(ends_rows(up, down, lane), tokens)
+
+
+def pack_body(mine, theirs, kept, far_out, out, sems):
     devices, part_rows, width = mine.shape
     spot = kept.shape[0] - 8
     tail = kept[spot : spot + 8][:GROUP].astype(BF)
+    step, writes = devices // 4, []
     for s in range(devices):
         rows = mine[s] + theirs[s].astype(F32)
         for k in range(part_rows // GROUP):
             group = rows[GROUP * k : GROUP * (k + 1)].astype(BF)
             out[s, :, width * k : width * (k + 1)] = group
         out[s, :, width * (part_rows // GROUP) :] = tail
-    write = pltpu.make_async_copy(out, far_out, sem)
-    write.start()
-    write.wait()
+        if (s + 1) % step == 0:
+            n = s // step
+            span = pl.ds(n * step, step)
+            writes.append(pltpu.make_async_copy(out.at[span], far_out.at[span], sems.at[n]))
+            writes[n].start()
+    for write in writes:
+        write.wait()
 
 
 def finish_body(last, saved, kept, g_proj, g_conv, g_branch, adds):
@@ -562,7 +568,7 @@
         pack_body,
         [((experts, GROUP, last_width), BF)],
         (mine, swapped, kept),
-        scratch=(pltpu.VMEM((experts, GROUP, last_width), BF), pltpu.SemaphoreType.DMA),
+        scratch=(pltpu.VMEM((experts, GROUP, last_width), BF), pltpu.SemaphoreType.DMA((4,))),
         far=(0,),
     )
     piece, acts = lax.optimization_barrier((piece, acts))

time: 165 us -> 165 us (level)
  no operation moved by 1% of the time
where the time goes in v5:
time: 165 us; the launch traced here: 164 us
  blocking collectives  129 us (78%)
  Pallas kernels  12.6 us (8%)
  waiting for transfers between devices  12.2 us (7%)
  starting transfers between devices  8.25 us (5%)
    all_to_all x1, blocking collectives, local(): whole = lax.all_to_all(spread, 'tp', 0, 0, tiled=True)  39.1 us
    all_to_all x1, blocking collectives, local(): got = lax.all_to_all(sent, 'sp', split_axis=0, concat_axis=0, tiled=True)  33.7 us
    all_to_all x1, blocking collectives, local(): lax.all_to_all(returned.reshape(experts, HOME_ROWS, lanes), 'sp', split_a...  24.4 us
    all_to_all x1, blocking collectives, local(): parts = lax.all_to_all(dxp, 'tp', 0, 0, tiled=True)  19.7 us
    all_to_all x1, blocking collectives, local(): lifted = lax.all_to_all(own, 'tp', 0, 0, tiled=True)  12.6 us
    all_to_all x1, waiting for transfers between devices, local(): last = lax.all_to_all(piece, 'sp', split_axis=0, concat_axis=0, tiled=True)  12.2 us
    pallas_call x9, Pallas kernels, call(): pl.pallas_call(body, out_shape=[pltpu.HBM(*out) if k in far else jax.Shap...  8.48 us
    ppermute x1, starting transfers between devices, local(): swapped = lax.ppermute(theirs, 'sp', [(i, i ^ 1) for i in range(experts)])  4.45 us
  transfers between devices with their start and end apart: 2, of which 1 were waited for; matrix products, arithmetic and copies ran while one was open for 0% of the time, Pallas kernels for 3%

profile of v5, /device:TPU:1, one launch (start us, length us, event | category | flops | bytes accessed | tf_op | source)
XLA Modules:
  0.0 164.1 jit_solution(16788728956820249399)
XLA Ops:
  0.6 1.4 shard_map.172
  2.0 33.7 %all_to_all.30.refs_0_ = bf16[32,4,640]{2,1,0:T(4,128)(2,1)S(1)} all-to-all(bf16[32,4,640]{2,1,0:T(4,128)(2,1)S(1)} %get-tuple-element.25), channel_id=1, replica_groups=mesh['sp'=32,'tp'=16] {'sp'}, dimensions={0} | all-to-all | bytes 327680 | tf_op jit(solution)/shard_map/all_to_all | solution.py:501
  35.7 0.7 shard_map.173
  36.4 0.0 copy-start
  36.4 0.0 copy-start.1
  36.4 0.0 copy-start.2
  36.4 39.1 %all_to_all.31.refs_5_.whole = bf16[16,640,128]{2,1,0:T(8,128)(2,1)S(1)} all-to-all(bf16[16,640,128]{2,1,0:T(8,128)(2,1)S(1)} %shard_map.173), channel_id=1, replica_groups=mesh['sp'=32,'tp'=16] {'tp'}, dimensions={0} | all-to-all | bytes 5242880 | tf_op jit(solution)/shard_map/all_to_all | solution.py:507
  75.5 0.0 copy-done
  75.5 0.0 copy-done.1
  75.5 0.0 copy-done.2
  75.5 2.4 %shard_map.174 = (bf16[16,320,128]{2,1,0:T(8,128)(2,1)S(1)}, bf16[320,384]{1,0:T(8,128)(2,1)}, f32[12,64,128]{2,1,0:T(8,128)S(1)}, bf16[8,128]{1,0:T(8,128)(2,1)S(1)}) custom-call(bf16[64,128]{1,0:T(8,128)(2,1)} %refs_0_.1, bf16[64,128]{1,0:T(8,128)(2,1)} %refs_1_.1, bf16[1,64,64]{2,1,0:T(8,128)(2,1)} %refs_2_.3, bf16[1,64,64]{2,1,0:T(8,128)(2,1)} %refs_3_.3, ...), custom_call_target="tpu_custom_call" | custom-call | flops 838860800 | bytes 1 | tf_op jit(solution)/shard_map/pallas_call | solution.py:39
  77.9 0.0 copy-start.4
  77.9 19.7 %all_to_all.32.refs_0_ = bf16[16,320,128]{2,1,0:T(8,128)(2,1)S(1)} all-to-all(bf16[16,320,128]{2,1,0:T(8,128)(2,1)S(1)} %get-tuple-element.26), channel_id=1, replica_groups=mesh['sp'=32,'tp'=16] {'tp'}, dimensions={0} | all-to-all | bytes 2621440 | tf_op jit(solution)/shard_map/all_to_all | solution.py:532
  97.6 0.0 copy-start.5
  97.6 0.5 shard_map.175
  98.0 24.4 %all_to_all.33 = bf16[32,16,128]{2,1,0:T(8,128)(2,1)S(1)} all-to-all(bf16[32,16,128]{2,1,0:T(8,128)(2,1)S(1)} %bitcast.12), channel_id=1, replica_groups=mesh['sp'=32,'tp'=16] {'sp'}, dimensions={0} | all-to-all | bytes 262144 | tf_op jit(solution)/shard_map/all_to_all | solution.py:538
  122.4 0.0 copy-done.4
  122.4 0.4 shard_map.176
  122.8 12.6 %all_to_all.34.lifted = bf16[16,128,128]{2,1,0:T(8,128)(2,1)S(1)} all-to-all(bf16[16,128,128]{2,1,0:T(8,128)(2,1)S(1)} %get-tuple-element.30), channel_id=1, replica_groups=mesh['sp'=32,'tp'=16] {'tp'}, dimensions={0} | all-to-all | bytes 1048576 | tf_op jit(solution)/shard_map/all_to_all | solution.py:551
  135.4 0.4 shard_map.177
  135.8 4.4 %collective-permute-start = (bf16[32,16,128]{2,1,0:T(8,128)(2,1)S(1)}, bf16[32,16,128]{2,1,0:T(8,128)(2,1)S(1)}, u32[]{:S(2)}, u32[]{:S(2)}) collective-permute-start(bf16[32,16,128]{2,1,0:T(8,128)(2,1)S(1)} %get-tuple-element.33), channel_id=1, source_target_pairs={{0,16},{16,0},{32,48},{48,32},{64,80},{80,64},{96,112},{112,96},{1... | collective-permute-start | bytes 393224 | tf_op jit(solution)/shard_map/ppermute | solution.py:560
  140.2 0.0 copy-done.5
  140.2 1.0 shard_map.178.kept
  141.2 0.0 collective-permute-done.theirs
  141.2 0.8 shard_map.179
  142.0 3.8 %all-to-all-start.5 = ((bf16[32,4,640]{2,1,0:T(4,128)(2,1)}), bf16[32,4,640]{2,1,0:T(4,128)(2,1)S(1)}, u32[]{:S(2)}, u32[]{:S(2)}) async-start(bf16[32,4,640]{2,1,0:T(4,128)(2,1)} %shard_map.179), calls=%async_computation.5 | async-start | bytes 327680 | tf_op jit(solution)/shard_map/all_to_all | solution.py:576
  145.8 0.0 copy-start.3
  145.8 0.9 copy-done.3
  146.8 4.1 %shard_map.180 = (bf16[1,128,2048]{2,1,0:T(8,128)(2,1)}, bf16[1,128,2048]{2,1,0:T(8,128)(2,1)}, bf16[1,128,2048]{2,1,0:T(8,128)(2,1)}) custom-call(bf16[16,640,128]{2,1,0:T(8,128)(2,1)S(1)} %all_to_all.31.refs_5_.whole, bf16[320,384]{1,0:T(8,128)(2,1)S(1)} %copy-done.3), custom_call_target="tpu_custom_call" | custom-call | flops 503316480 | bytes 1572864 | tf_op jit(solution)/shard_map/pallas_call | solution.py:187
  150.8 12.2 %all-to-all-done.5.last = bf16[32,4,640]{2,1,0:T(4,128)(2,1)S(1)} async-done(((bf16[32,4,640]{2,1,0:T(4,128)(2,1)}), bf16[32,4,640]{2,1,0:T(4,128)(2,1)S(1)}, u32[]{:S(2)}, u32[]{:S(2)}) %all-to-all-start.5) | async-done | bytes 163872 | tf_op jit(solution)/shard_map/all_to_all | solution.py:576
  163.0 1.1 shard_map.181
Async XLA Ops:
  36.4 39.1 %copy-start = (bf16[1,128,2048]{2,1,0:T(8,128)(2,1)S(1)}, bf16[1,128,2048]{2,1,0:T(8,128)(2,1)}, u32[]{:S(2)}) copy-start(bf16[1,128,2048]{2,1,0:T(8,128)(2,1)} %param.17) | copy-start | bytes 1572868
  36.4 39.1 %copy-start.1 = (bf16[1,128,2048]{2,1,0:T(8,128)(2,1)S(1)}, bf16[1,128,2048]{2,1,0:T(8,128)(2,1)}, u32[]{:S(2)}) copy-start(bf16[1,128,2048]{2,1,0:T(8,128)(2,1)} %param.18) | copy-start | bytes 1572868
  36.4 39.1 %copy-start.2 = (bf16[1,128,2048]{2,1,0:T(8,128)(2,1)S(1)}, bf16[1,128,2048]{2,1,0:T(8,128)(2,1)}, u32[]{:S(2)}) copy-start(bf16[1,128,2048]{2,1,0:T(8,128)(2,1)} %param.19) | copy-start | bytes 1572868
  77.9 44.5 %copy-start.4 = (bf16[128,128]{1,0:T(8,128)(2,1)S(1)}, bf16[128,128]{1,0:T(8,128)(2,1)}, u32[]{:S(2)}) copy-start(bf16[128,128]{1,0:T(8,128)(2,1)} %cot.1) | copy-start | bytes 98308
  97.6 42.7 %copy-start.5 = (bf16[64,2048]{1,0:T(8,128)(2,1)S(1)}, bf16[64,2048]{1,0:T(8,128)(2,1)}, u32[]{:S(2)}) copy-start(bf16[64,2048]{1,0:T(8,128)(2,1)} %w_out.1) | copy-start | bytes 786436
  135.8 5.5 %collective-permute-start = (bf16[32,16,128]{2,1,0:T(8,128)(2,1)S(1)}, bf16[32,16,128]{2,1,0:T(8,128)(2,1)S(1)}, u32[]{:S(2)}, u32[]{:S(2)}) collective-permute-start(bf16[32,16,128]{2,1,0:T(8,128)(2,1)S(1)} %get-tuple-element.33), channel_id=1, source_target_pairs={{0,16},{16,0},{32,48},{48,32},{64,80},{80,64},{96,112},{112,96},{1... | collective-permute-start | bytes 393224 | tf_op jit(solution)/shard_map/ppermute | solution.py:560
  142.0 21.0 %all-to-all-start.5 = ((bf16[32,4,640]{2,1,0:T(4,128)(2,1)}), bf16[32,4,640]{2,1,0:T(4,128)(2,1)S(1)}, u32[]{:S(2)}, u32[]{:S(2)}) async-start(bf16[32,4,640]{2,1,0:T(4,128)(2,1)} %shard_map.179), calls=%async_computation.5 | async-start | bytes 327680 | tf_op jit(solution)/shard_map/all_to_all | solution.py:576
  145.8 0.9 copy-start.3

commit v6 on v5

--- a/solution.py
+++ b/solution.py
@@ -131,11 +131,23 @@
     return jnp.concatenate([ref[2 * k, lo:hi, :], ref[2 * k + 1, lo:hi, :]], axis=1)
 
 
-def expert_body(*refs):
-    sources, (whole, w_gate, w_up, w_down) = refs[:5], refs[5:9]
-    dxp, far_acts, saved, carry = refs[9:13]
-    targets, acts, acts_sem, sems = refs[13:18], refs[18], refs[19], refs[20]
-    copies = fetch(sources, targets, sems)
+def expert_body(
+    conv,
+    branch,
+    w_recur,
+    w_input,
+    decay_param,
+    whole,
+    w_gate,
+    w_up,
+    w_down,
+    dxp,
+    far_acts,
+    saved,
+    carry,
+    acts,
+    acts_sem,
+):
     slots = whole.shape[1] // 2
     blocks = whole.shape[0]
     hidden = w_gate.shape[0]
@@ -146,6 +158,7 @@
         both = jnp.concatenate([w_gate[:, cols], w_up[:, cols]], axis=0)
         pre = pre + dot(pair(whole, k, 0, slots), both, 1, 1)
         act_cot = act_cot + dot(pair(whole, k, slots, 2 * slots), w_down[:, cols], 1, 1)
+    state_body(conv, branch, w_recur, w_input, decay_param, saved, carry)
     pre_gate, pre_up = pre[:, :hidden], pre[:, hidden:]
     sig = jax.nn.sigmoid(pre_gate)
     silu = pre_gate * sig
@@ -164,9 +177,6 @@
         part = dot(cots, both).astype(BF)
         dxp[2 * k] = part[:, :128]
         dxp[2 * k + 1] = part[:, 128:]
-    for copy in copies:
-        copy.wait()
-    state_body(*targets, saved, carry)
     write.wait()
 
 
@@ -524,7 +534,6 @@
             w_up[0],
             w_down[0],
         ),
-        fetched=5,
         scratch=(pltpu.VMEM((slots, 3 * hidden), BF), pltpu.SemaphoreType.DMA),
         far=(1,),
         flops=10 * slots * hidden * width,

time: 165 us -> 164 us (level)
  no operation moved by 1% of the time
where the time goes in v6:
time: 164 us
  blocking collectives  129 us (79%)
  Pallas kernels  12.2 us (7%)
  waiting for transfers between devices  12.2 us (7%)
  starting transfers between devices  8.25 us (5%)
    all_to_all x1, blocking collectives, local(): whole = lax.all_to_all(spread, 'tp', 0, 0, tiled=True)  39.1 us
    all_to_all x1, blocking collectives, local(): got = lax.all_to_all(sent, 'sp', split_axis=0, concat_axis=0, tiled=True)  33.7 us
    all_to_all x1, blocking collectives, local(): lax.all_to_all(returned.reshape(experts, HOME_ROWS, lanes), 'sp', split_a...  24.4 us
    all_to_all x1, blocking collectives, local(): parts = lax.all_to_all(dxp, 'tp', 0, 0, tiled=True)  19.7 us
    all_to_all x1, blocking collectives, local(): lifted = lax.all_to_all(own, 'tp', 0, 0, tiled=True)  12.6 us
    all_to_all x1, waiting for transfers between devices, local(): last = lax.all_to_all(piece, 'sp', split_axis=0, concat_axis=0, tiled=True)  12.2 us
    pallas_call x9, Pallas kernels, call(): pl.pallas_call(body, out_shape=[pltpu.HBM(*out) if k in far else jax.Shap...  8.05 us
    ppermute x1, starting transfers between devices, local(): swapped = lax.ppermute(theirs, 'sp', [(i, i ^ 1) for i in range(experts)])  4.45 us
  transfers between devices with their start and end apart: 2, of which 1 were waited for; matrix products, arithmetic and copies ran while one was open for 0% of the time, Pallas kernels for 3%

profile of v6, /device:TPU:1, one launch (start us, length us, event | category | flops | bytes accessed | tf_op | source)
XLA Modules:
  0.0 163.8 jit_solution(1412285650645343588)
XLA Ops:
  0.6 1.4 shard_map.172
  2.0 33.7 %all_to_all.30.refs_0_ = bf16[32,4,640]{2,1,0:T(4,128)(2,1)S(1)} all-to-all(bf16[32,4,640]{2,1,0:T(4,128)(2,1)S(1)} %get-tuple-element.25), channel_id=1, replica_groups=mesh['sp'=32,'tp'=16] {'sp'}, dimensions={0} | all-to-all | bytes 327680 | tf_op jit(solution)/shard_map/all_to_all | solution.py:511
  35.7 0.7 shard_map.173
  36.4 0.0 copy-start
  36.4 0.0 copy-start.1
  36.4 0.0 copy-start.2
  36.4 0.0 copy-start.5
  36.4 0.0 copy-start.6
  36.4 0.0 copy-start.7
  36.4 0.0 copy-start.8
  36.5 0.0 copy-start.9
  36.5 39.1 %all_to_all.31.whole = bf16[16,640,128]{2,1,0:T(8,128)(2,1)S(1)} all-to-all(bf16[16,640,128]{2,1,0:T(8,128)(2,1)S(1)} %shard_map.173), channel_id=1, replica_groups=mesh['sp'=32,'tp'=16] {'tp'}, dimensions={0} | all-to-all | bytes 5242880 | tf_op jit(solution)/shard_map/all_to_all | solution.py:517
  75.5 0.0 copy-done
  75.5 0.0 copy-done.1
  75.5 0.0 copy-done.2
  75.5 0.0 copy-done.5
  75.5 0.0 copy-done.6
  75.5 0.0 copy-done.7
  75.6 0.0 copy-done.8
  75.6 0.0 copy-done.9
  75.6 2.0 %shard_map.174 = (bf16[16,320,128]{2,1,0:T(8,128)(2,1)S(1)}, bf16[320,384]{1,0:T(8,128)(2,1)}, f32[12,64,128]{2,1,0:T(8,128)S(1)}, bf16[8,128]{1,0:T(8,128)(2,1)S(1)}) custom-call(bf16[64,128]{1,0:T(8,128)(2,1)S(1)} %copy-done.5, bf16[64,128]{1,0:T(8,128)(2,1)S(1)} %copy-done.6, bf16[1,64,64]{2,1,0:T(8,128)(2,1)S(1)} %copy-done.7, ...), custom_call_target="tpu_custom_call" | custom-call | flops 838860800 | bytes 1 | tf_op jit(solution)/shard_map/pallas_call | solution.py:39
  77.6 0.0 copy-start.4
  77.6 19.7 %all_to_all.32.refs_0_ = bf16[16,320,128]{2,1,0:T(8,128)(2,1)S(1)} all-to-all(bf16[16,320,128]{2,1,0:T(8,128)(2,1)S(1)} %get-tuple-element.26), channel_id=1, replica_groups=mesh['sp'=32,'tp'=16] {'tp'}, dimensions={0} | all-to-all | bytes 2621440 | tf_op jit(solution)/shard_map/all_to_all | solution.py:541
  97.3 0.0 copy-start.10
  97.3 0.5 shard_map.175
  97.7 24.4 %all_to_all.33 = bf16[32,16,128]{2,1,0:T(8,128)(2,1)S(1)} all-to-all(bf16[32,16,128]{2,1,0:T(8,128)(2,1)S(1)} %bitcast.12), channel_id=1, replica_groups=mesh['sp'=32,'tp'=16] {'sp'}, dimensions={0} | all-to-all | bytes 262144 | tf_op jit(solution)/shard_map/all_to_all | solution.py:547
  122.1 0.0 copy-done.4
  122.1 0.4 shard_map.176
  122.5 12.6 %all_to_all.34.lifted = bf16[16,128,128]{2,1,0:T(8,128)(2,1)S(1)} all-to-all(bf16[16,128,128]{2,1,0:T(8,128)(2,1)S(1)} %get-tuple-element.30), channel_id=1, replica_groups=mesh['sp'=32,'tp'=16] {'tp'}, dimensions={0} | all-to-all | bytes 1048576 | tf_op jit(solution)/shard_map/all_to_all | solution.py:560
  135.1 0.4 shard_map.177
  135.5 4.4 %collective-permute-start = (bf16[32,16,128]{2,1,0:T(8,128)(2,1)S(1)}, bf16[32,16,128]{2,1,0:T(8,128)(2,1)S(1)}, u32[]{:S(2)}, u32[]{:S(2)}) collective-permute-start(bf16[32,16,128]{2,1,0:T(8,128)(2,1)S(1)} %get-tuple-element.33), channel_id=1, source_target_pairs={{0,16},{16,0},{32,48},{48,32},{64,80},{80,64},{96,112},{112,96},{1... | collective-permute-start | bytes 393224 | tf_op jit(solution)/shard_map/ppermute | solution.py:569
  139.9 0.0 copy-done.10
  139.9 1.0 shard_map.178.kept
  140.9 0.0 collective-permute-done.theirs
  140.9 0.7 shard_map.179
  141.7 3.8 %all-to-all-start.5 = ((bf16[32,4,640]{2,1,0:T(4,128)(2,1)}), bf16[32,4,640]{2,1,0:T(4,128)(2,1)S(1)}, u32[]{:S(2)}, u32[]{:S(2)}) async-start(bf16[32,4,640]{2,1,0:T(4,128)(2,1)} %shard_map.179), calls=%async_computation.5 | async-start | bytes 327680 | tf_op jit(solution)/shard_map/all_to_all | solution.py:585
  145.5 0.0 copy-start.3
  145.5 0.9 copy-done.3
  146.4 4.1 %shard_map.180 = (bf16[1,128,2048]{2,1,0:T(8,128)(2,1)}, bf16[1,128,2048]{2,1,0:T(8,128)(2,1)}, bf16[1,128,2048]{2,1,0:T(8,128)(2,1)}) custom-call(bf16[16,640,128]{2,1,0:T(8,128)(2,1)S(1)} %all_to_all.31.whole, bf16[320,384]{1,0:T(8,128)(2,1)S(1)} %copy-done.3), custom_call_target="tpu_custom_call" | custom-call | flops 503316480 | bytes 1572864 | tf_op jit(solution)/shard_map/pallas_call | solution.py:197
  150.5 12.2 %all-to-all-done.5.last = bf16[32,4,640]{2,1,0:T(4,128)(2,1)S(1)} async-done(((bf16[32,4,640]{2,1,0:T(4,128)(2,1)}), bf16[32,4,640]{2,1,0:T(4,128)(2,1)S(1)}, u32[]{:S(2)}, u32[]{:S(2)}) %all-to-all-start.5) | async-done | bytes 163872 | tf_op jit(solution)/shard_map/all_to_all | solution.py:585
  162.7 1.1 shard_map.181
Async XLA Ops:
  36.4 39.2 %copy-start = (bf16[1,128,2048]{2,1,0:T(8,128)(2,1)S(1)}, bf16[1,128,2048]{2,1,0:T(8,128)(2,1)}, u32[]{:S(2)}) copy-start(bf16[1,128,2048]{2,1,0:T(8,128)(2,1)} %param.17) | copy-start | bytes 1572868
  36.4 39.1 %copy-start.1 = (bf16[1,128,2048]{2,1,0:T(8,128)(2,1)S(1)}, bf16[1,128,2048]{2,1,0:T(8,128)(2,1)}, u32[]{:S(2)}) copy-start(bf16[1,128,2048]{2,1,0:T(8,128)(2,1)} %param.18) | copy-start | bytes 1572868
  36.4 39.1 %copy-start.2 = (bf16[1,128,2048]{2,1,0:T(8,128)(2,1)S(1)}, bf16[1,128,2048]{2,1,0:T(8,128)(2,1)}, u32[]{:S(2)}) copy-start(bf16[1,128,2048]{2,1,0:T(8,128)(2,1)} %param.19) | copy-start | bytes 1572868
  36.4 39.1 %copy-start.5 = (bf16[64,128]{1,0:T(8,128)(2,1)S(1)}, bf16[64,128]{1,0:T(8,128)(2,1)}, u32[]{:S(2)}) copy-start(bf16[64,128]{1,0:T(8,128)(2,1)} %conv.1) | copy-start | bytes 49156
  36.4 39.1 %copy-start.6 = (bf16[64,128]{1,0:T(8,128)(2,1)S(1)}, bf16[64,128]{1,0:T(8,128)(2,1)}, u32[]{:S(2)}) copy-start(bf16[64,128]{1,0:T(8,128)(2,1)} %branch.1) | copy-start | bytes 49156
  36.4 39.1 %copy-start.7 = (bf16[1,64,64]{2,1,0:T(8,128)(2,1)S(1)}, bf16[1,64,64]{2,1,0:T(8,128)(2,1)}, u32[]{:S(2)}) copy-start(bf16[1,64,64]{2,1,0:T(8,128)(2,1)} %w_recur.1) | copy-start | bytes 24580
  36.4 39.1 %copy-start.8 = (bf16[1,64,64]{2,1,0:T(8,128)(2,1)S(1)}, bf16[1,64,64]{2,1,0:T(8,128)(2,1)}, u32[]{:S(2)}) copy-start(bf16[1,64,64]{2,1,0:T(8,128)(2,1)} %w_input.1) | copy-start | bytes 24580
  36.5 39.1 %copy-start.9 = (f32[64]{0:T(128)S(1)}, f32[64]{0:T(128)}, u32[]{:S(2)}) copy-start(f32[64]{0:T(128)} %param.25) | copy-start | bytes 772
  77.6 44.5 %copy-start.4 = (bf16[128,128]{1,0:T(8,128)(2,1)S(1)}, bf16[128,128]{1,0:T(8,128)(2,1)}, u32[]{:S(2)}) copy-start(bf16[128,128]{1,0:T(8,128)(2,1)} %cot.1) | copy-start | bytes 98308
  97.3 42.7 %copy-start.10 = (bf16[64,2048]{1,0:T(8,128)(2,1)S(1)}, bf16[64,2048]{1,0:T(8,128)(2,1)}, u32[]{:S(2)}) copy-start(bf16[64,2048]{1,0:T(8,128)(2,1)} %w_out.1) | copy-start | bytes 786436
  135.5 5.5 %collective-permute-start = (bf16[32,16,128]{2,1,0:T(8,128)(2,1)S(1)}, bf16[32,16,128]{2,1,0:T(8,128)(2,1)S(1)}, u32[]{:S(2)}, u32[]{:S(2)}) collective-permute-start(bf16[32,16,128]{2,1,0:T(8,128)(2,1)S(1)} %get-tuple-element.33), channel_id=1, source_target_pairs={{0,16},{16,0},{32,48},{48,32},{64,80},{80,64},{96,112},{112,96},{1... | collective-permute-start | bytes 393224 | tf_op jit(solution)/shard_map/ppermute | solution.py:569
  141.7 21.0 %all-to-all-start.5 = ((bf16[32,4,640]{2,1,0:T(4,128)(2,1)}), bf16[32,4,640]{2,1,0:T(4,128)(2,1)S(1)}, u32[]{:S(2)}, u32[]{:S(2)}) async-start(bf16[32,4,640]{2,1,0:T(4,128)(2,1)} %shard_map.179), calls=%async_computation.5 | async-start | bytes 327680 | tf_op jit(solution)/shard_map/all_to_all | solution.py:585
  145.5 0.9 copy-start.3

commit v7 on v6

--- a/solution.py
+++ b/solution.py
@@ -142,11 +142,9 @@
     w_up,
     w_down,
     dxp,
-    far_acts,
+    acts,
     saved,
     carry,
-    acts,
-    acts_sem,
 ):
     slots = whole.shape[1] // 2
     blocks = whole.shape[0]
@@ -169,15 +167,12 @@
     cots = jnp.concatenate([gate_cot, up_cot], axis=1)
     acts[:, : 2 * hidden] = cots
     acts[:, 2 * hidden :] = act
-    write = pltpu.make_async_copy(acts, far_acts, acts_sem)
-    write.start()
     for k in range(blocks // 2):
         cols = slice(256 * k, 256 * (k + 1))
         both = jnp.concatenate([w_gate[:, cols], w_up[:, cols]], axis=0)
         part = dot(cots, both).astype(BF)
         dxp[2 * k] = part[:, :128]
         dxp[2 * k + 1] = part[:, 128:]
-    write.wait()
 
 
 def grads_body(whole, acts, g_gate, g_up, g_down):
@@ -210,7 +205,7 @@
     )(whole, acts)
 
 
-def owner_sum_body(experts, capacity, parts, carry, out):
+def owner_sum_body(experts, capacity, parts, carry, acts, out):
     total = parts[0].astype(F32)
     for j in range(1, parts.shape[0]):
         total = total + parts[j].astype(F32)
@@ -534,15 +529,13 @@
             w_up[0],
             w_down[0],
         ),
-        scratch=(pltpu.VMEM((slots, 3 * hidden), BF), pltpu.SemaphoreType.DMA),
-        far=(1,),
         flops=10 * slots * hidden * width,
     )
     parts = lax.all_to_all(dxp, "tp", 0, 0, tiled=True)
     (returned,) = call(
         kernel(owner_sum_body, experts, capacity),
         [((experts * HOME_ROWS, lanes), BF)],
-        (parts, carry),
+        (parts, carry, acts),
     )
     home = lax.all_to_all(
         returned.reshape(experts, HOME_ROWS, lanes), "sp", split_axis=0, concat_axis=0, tiled=True

time: 164 us -> 166 us (1.012)
  no operation moved by 1% of the time
where the time goes in v7:
time: 166 us; the launch traced here: 165 us
  blocking collectives  129 us (78%)
  waiting for transfers between devices  13.2 us (8%)
  Pallas kernels  13.1 us (8%)
  starting transfers between devices  8.9 us (5%)
    all_to_all x1, blocking collectives, local(): whole = lax.all_to_all(spread, 'tp', 0, 0, tiled=True)  39.1 us
    all_to_all x1, blocking collectives, local(): got = lax.all_to_all(sent, 'sp', split_axis=0, concat_axis=0, tiled=True)  33.7 us
    all_to_all x1, blocking collectives, local(): lax.all_to_all(returned.reshape(experts, HOME_ROWS, lanes), 'sp', split_a...  24.4 us
    all_to_all x1, blocking collectives, local(): parts = lax.all_to_all(dxp, 'tp', 0, 0, tiled=True)  19.7 us
    all_to_all x1, waiting for transfers between devices, local(): last = lax.all_to_all(piece, 'sp', split_axis=0, concat_axis=0, tiled=True)  13.1 us
    all_to_all x1, blocking collectives, local(): lifted = lax.all_to_all(own, 'tp', 0, 0, tiled=True)  12.6 us
    pallas_call x9, Pallas kernels, call(): pl.pallas_call(body, out_shape=[pltpu.HBM(*out) if k in far else jax.Shap...  8.97 us
    ppermute x1, starting transfers between devices, local(): swapped = lax.ppermute(theirs, 'sp', [(i, i ^ 1) for i in range(experts)])  4.46 us
  transfers between devices with their start and end apart: 2, of which 1 were waited for; matrix products, arithmetic and copies ran while one was open for 0% of the time, Pallas kernels for 3%

profile of v7, /device:TPU:1, one launch (start us, length us, event | category | flops | bytes accessed | tf_op | source)
XLA Modules:
  0.0 165.4 jit_solution(8063319655201474002)
XLA Ops:
  0.6 1.4 shard_map.172
  2.0 33.7 %all_to_all.30.refs_0_ = bf16[32,4,640]{2,1,0:T(4,128)(2,1)S(1)} all-to-all(bf16[32,4,640]{2,1,0:T(4,128)(2,1)S(1)} %get-tuple-element.25), channel_id=1, replica_groups=mesh['sp'=32,'tp'=16] {'sp'}, dimensions={0} | all-to-all | bytes 327680 | tf_op jit(solution)/shard_map/all_to_all | solution.py:506
  35.7 0.7 shard_map.173
  36.4 0.0 copy-start
  36.4 0.0 copy-start.1
  36.4 0.0 copy-start.2
  36.4 0.0 copy-start.4
  36.4 0.0 copy-start.5
  36.4 0.0 copy-start.6
  36.4 0.0 copy-start.7
  36.5 0.0 copy-start.8
  36.5 39.1 %all_to_all.31.whole = bf16[16,640,128]{2,1,0:T(8,128)(2,1)S(1)} all-to-all(bf16[16,640,128]{2,1,0:T(8,128)(2,1)S(1)} %shard_map.173), channel_id=1, replica_groups=mesh['sp'=32,'tp'=16] {'tp'}, dimensions={0} | all-to-all | bytes 5242880 | tf_op jit(solution)/shard_map/all_to_all | solution.py:512
  75.5 0.0 copy-done
  75.5 0.0 copy-done.1
  75.5 0.0 copy-done.2
  75.5 0.0 copy-done.4
  75.5 0.0 copy-done.5
  75.6 0.0 copy-done.6
  75.6 0.0 copy-done.7
  75.6 0.0 copy-done.8
  75.6 2.0 %shard_map.174 = (bf16[16,320,128]{2,1,0:T(8,128)(2,1)S(1)}, bf16[320,384]{1,0:T(8,128)(2,1)S(1)}, f32[12,64,128]{2,1,0:T(8,128)S(1)}, bf16[8,128]{1,0:T(8,128)(2,1)S(1)}) custom-call(bf16[64,128]{1,0:T(8,128)(2,1)S(1)} %copy-done.4, bf16[64,128]{1,0:T(8,128)(2,1)S(1)} %copy-done.5, bf16[1,64,64]{2,1,0:T(8,128)(2,1)S(1)} %copy-done.6, ...), custom_call_target="tpu_custom_call" | custom-call | flops 838860800 | bytes 1 | tf_op jit(solution)/shard_map/pallas_call | solution.py:39
  77.6 0.0 copy-start.3
  77.6 19.7 %all_to_all.32.refs_0_ = bf16[16,320,128]{2,1,0:T(8,128)(2,1)S(1)} all-to-all(bf16[16,320,128]{2,1,0:T(8,128)(2,1)S(1)} %get-tuple-element.26), channel_id=1, replica_groups=mesh['sp'=32,'tp'=16] {'tp'}, dimensions={0} | all-to-all | bytes 2621440 | tf_op jit(solution)/shard_map/all_to_all | solution.py:534
  97.2 0.0 copy-start.9
  97.2 0.5 shard_map.175
  97.7 24.4 %all_to_all.33 = bf16[32,16,128]{2,1,0:T(8,128)(2,1)S(1)} all-to-all(bf16[32,16,128]{2,1,0:T(8,128)(2,1)S(1)} %bitcast.11), channel_id=1, replica_groups=mesh['sp'=32,'tp'=16] {'sp'}, dimensions={0} | all-to-all | bytes 262144 | tf_op jit(solution)/shard_map/all_to_all | solution.py:540
  122.1 0.0 copy-done.3
  122.1 0.4 shard_map.176
  122.5 12.6 %all_to_all.34.lifted = bf16[16,128,128]{2,1,0:T(8,128)(2,1)S(1)} all-to-all(bf16[16,128,128]{2,1,0:T(8,128)(2,1)S(1)} %get-tuple-element.31), channel_id=1, replica_groups=mesh['sp'=32,'tp'=16] {'tp'}, dimensions={0} | all-to-all | bytes 1048576 | tf_op jit(solution)/shard_map/all_to_all | solution.py:553
  135.1 0.4 shard_map.177
  135.4 4.5 %collective-permute-start = (bf16[32,16,128]{2,1,0:T(8,128)(2,1)S(1)}, bf16[32,16,128]{2,1,0:T(8,128)(2,1)S(1)}, u32[]{:S(2)}, u32[]{:S(2)}) collective-permute-start(bf16[32,16,128]{2,1,0:T(8,128)(2,1)S(1)} %get-tuple-element.34), channel_id=1, source_target_pairs={{0,16},{16,0},{32,48},{48,32},{64,80},{80,64},{96,112},{112,96},{1... | collective-permute-start | bytes 393224 | tf_op jit(solution)/shard_map/ppermute | solution.py:562
  139.9 0.0 copy-done.9
  139.9 1.0 shard_map.178.kept
  140.9 0.0 collective-permute-done.theirs
  140.9 0.8 shard_map.179
  141.7 4.4 %all-to-all-start.5 = ((bf16[32,4,640]{2,1,0:T(4,128)(2,1)}), bf16[32,4,640]{2,1,0:T(4,128)(2,1)}, u32[]{:S(2)}, u32[]{:S(2)}) async-start(bf16[32,4,640]{2,1,0:T(4,128)(2,1)} %shard_map.179), calls=%async_computation.5 | async-start | bytes 327680 | tf_op jit(solution)/shard_map/all_to_all | solution.py:578
  146.1 4.1 %shard_map.180 = (bf16[1,128,2048]{2,1,0:T(8,128)(2,1)}, bf16[1,128,2048]{2,1,0:T(8,128)(2,1)}, bf16[1,128,2048]{2,1,0:T(8,128)(2,1)}) custom-call(bf16[16,640,128]{2,1,0:T(8,128)(2,1)S(1)} %all_to_all.31.whole, bf16[320,384]{1,0:T(8,128)(2,1)S(1)} %get-tuple-element.36.refs_2_.acts), custom_call_target="tpu_custom_call" | custom-call | flops 503316480 | bytes 1572864 | tf_op jit(solution)/shard_map/pallas_call | solution.py:192
  150.3 13.1 %all-to-all-done.5.last = bf16[32,4,640]{2,1,0:T(4,128)(2,1)} async-done(((bf16[32,4,640]{2,1,0:T(4,128)(2,1)}), bf16[32,4,640]{2,1,0:T(4,128)(2,1)}, u32[]{:S(2)}, u32[]{:S(2)}) %all-to-all-start.5) | async-done | bytes 163872 | tf_op jit(solution)/shard_map/all_to_all | solution.py:578
  163.4 2.0 %shard_map.181 = (f32[64,64]{1,0:T(8,128)}, f32[64,128]{1,0:T(8,128)}, f32[64,128]{1,0:T(8,128)}) custom-call(bf16[32,4,640]{2,1,0:T(4,128)(2,1)} %all-to-all-done.5.last, f32[12,64,128]{2,1,0:T(8,128)S(1)} %get-tuple-element.30.saved, f32[384,128]{1,0:T(8,128)S(1)} %shard_map.178.kept), custom_call_target="tpu_custom_call" | custom-call | flops 1 | bytes 1 | tf_op jit(solution)/shard_map/pallas_call | solution.py:39
Async XLA Ops:
  36.4 39.2 %copy-start = (bf16[1,128,2048]{2,1,0:T(8,128)(2,1)S(1)}, bf16[1,128,2048]{2,1,0:T(8,128)(2,1)}, u32[]{:S(2)}) copy-start(bf16[1,128,2048]{2,1,0:T(8,128)(2,1)} %param.17) | copy-start | bytes 1572868
  36.4 39.1 %copy-start.1 = (bf16[1,128,2048]{2,1,0:T(8,128)(2,1)S(1)}, bf16[1,128,2048]{2,1,0:T(8,128)(2,1)}, u32[]{:S(2)}) copy-start(bf16[1,128,2048]{2,1,0:T(8,128)(2,1)} %param.18) | copy-start | bytes 1572868
  36.4 39.1 %copy-start.2 = (bf16[1,128,2048]{2,1,0:T(8,128)(2,1)S(1)}, bf16[1,128,2048]{2,1,0:T(8,128)(2,1)}, u32[]{:S(2)}) copy-start(bf16[1,128,2048]{2,1,0:T(8,128)(2,1)} %param.19) | copy-start | bytes 1572868
  36.4 39.1 %copy-start.4 = (bf16[64,128]{1,0:T(8,128)(2,1)S(1)}, bf16[64,128]{1,0:T(8,128)(2,1)}, u32[]{:S(2)}) copy-start(bf16[64,128]{1,0:T(8,128)(2,1)} %conv.1) | copy-start | bytes 49156
  36.4 39.1 %copy-start.5 = (bf16[64,128]{1,0:T(8,128)(2,1)S(1)}, bf16[64,128]{1,0:T(8,128)(2,1)}, u32[]{:S(2)}) copy-start(bf16[64,128]{1,0:T(8,128)(2,1)} %branch.1) | copy-start | bytes 49156
  36.4 39.1 %copy-start.6 = (bf16[1,64,64]{2,1,0:T(8,128)(2,1)S(1)}, bf16[1,64,64]{2,1,0:T(8,128)(2,1)}, u32[]{:S(2)}) copy-start(bf16[1,64,64]{2,1,0:T(8,128)(2,1)} %w_recur.1) | copy-start | bytes 24580
  36.4 39.1 %copy-start.7 = (bf16[1,64,64]{2,1,0:T(8,128)(2,1)S(1)}, bf16[1,64,64]{2,1,0:T(8,128)(2,1)}, u32[]{:S(2)}) copy-start(bf16[1,64,64]{2,1,0:T(8,128)(2,1)} %w_input.1) | copy-start | bytes 24580
  36.5 39.1 %copy-start.8 = (f32[64]{0:T(128)S(1)}, f32[64]{0:T(128)}, u32[]{:S(2)}) copy-start(f32[64]{0:T(128)} %param.25) | copy-start | bytes 772
  77.6 44.5 %copy-start.3 = (bf16[128,128]{1,0:T(8,128)(2,1)S(1)}, bf16[128,128]{1,0:T(8,128)(2,1)}, u32[]{:S(2)}) copy-start(bf16[128,128]{1,0:T(8,128)(2,1)} %cot.1) | copy-start | bytes 98308
  97.2 42.7 %copy-start.9 = (bf16[64,2048]{1,0:T(8,128)(2,1)S(1)}, bf16[64,2048]{1,0:T(8,128)(2,1)}, u32[]{:S(2)}) copy-start(bf16[64,2048]{1,0:T(8,128)(2,1)} %w_out.1) | copy-start | bytes 786436
  135.4 5.5 %collective-permute-start = (bf16[32,16,128]{2,1,0:T(8,128)(2,1)S(1)}, bf16[32,16,128]{2,1,0:T(8,128)(2,1)S(1)}, u32[]{:S(2)}, u32[]{:S(2)}) collective-permute-start(bf16[32,16,128]{2,1,0:T(8,128)(2,1)S(1)} %get-tuple-element.34), channel_id=1, source_target_pairs={{0,16},{16,0},{32,48},{48,32},{64,80},{80,64},{96,112},{112,96},{1... | collective-permute-start | bytes 393224 | tf_op jit(solution)/shard_map/ppermute | solution.py:562
  141.7 21.7 %all-to-all-start.5 = ((bf16[32,4,640]{2,1,0:T(4,128)(2,1)}), bf16[32,4,640]{2,1,0:T(4,128)(2,1)}, u32[]{:S(2)}, u32[]{:S(2)}) async-start(bf16[32,4,640]{2,1,0:T(4,128)(2,1)} %shard_map.179), calls=%async_computation.5 | async-start | bytes 327680 | tf_op jit(solution)/shard_map/all_to_all | solution.py:578
